TPU v7x, 128 devices: a whole 4x4x4 slice. The times are simulated.
128 devices in a mesh: kv: 32 (over z, y, core), tp: 4 (over x).
Axes of the slice: x: 4, y: 4, z: 4, core: 2. Of those that a mesh axis runs over, the one named last changes fastest.
Arguments:
- layer_input: bfloat16 [4, 16384, 2048], P(None, 'kv', 'tp'), may hold values from -0.119628906 to 0.119628906
- queries: bfloat16 [4, 16384, 2048], P(None, 'kv', 'tp'), may hold values from -3.5 to 3.5
- keys: bfloat16 [4, 16384, 2048], P(None, 'kv', 'tp'), may hold values from -3.5 to 3.5
- values: bfloat16 [4, 16384, 2048], P(None, 'kv', 'tp'), may hold values from -5 to 5
- outputs: bfloat16 [4, 16384, 2048], P(None, 'kv', 'tp'), may hold values from -1.5 to 1.5
- d_out: bfloat16 [4, 16384, 2048], P(None, 'kv', 'tp'), may hold values from -30 to 30
- log_sums: float32 [4, 16384, 16], P(None, 'kv', 'tp'), may hold values from 6 to 8
- chosen: int32 [4, 256, 12], P(None, 'kv'), may hold values from -1 to 255, as said below
Outputs:
- d_queries: bfloat16 [4, 16384, 2048], P(None, 'kv', 'tp')
- d_keys: bfloat16 [4, 16384, 2048], P(None, 'kv', 'tp')
- d_values: bfloat16 [4, 16384, 2048], P(None, 'kv', 'tp')
- d_weight: float32 [2048, 2048], P('kv', 'tp')
Inputs may be any that keep to these rules, and one draw needn't show every extreme that they name: Row chosen[s, b] names key blocks of sequence s for query block b: its first entry is b itself, the others are distinct blocks with smaller indices, either on the same device as b or on earlier devices; -1 marks unused slots, which come last. Over all sequences, the blocks of one device that query blocks of other devices name are at most 2, and in every draw some devices' are exactly 2.
All inputs are finite; a program needn't handle non-finite values.
Results may differ from a plain program's by a relative error of at most 0.0055.
Values may be sent and summed in bfloat16 or wider, within the bound.
A program may use at most 256 MiB of HBM per device.

v0:
```python
import jax
import jax.numpy as jnp
from jax import lax
from jax.sharding import PartitionSpec as P

BLK = 64
SEL = 12
CAP = 2


def over_pieces(shard, axis):
    blocks = lax.all_gather(shard, axis)
    return blocks.max(axis=0)


def in_one_piece(arrays, axis, dim, along):
    both = jnp.concatenate(arrays, axis=along)
    whole, at, gathered = (lax.all_gather(both, axis, axis=dim, tiled=True), 0, [])
    for a in arrays:
        gathered.append(lax.slice_in_dim(whole, at, at + a.shape[along], axis=along))
        at += a.shape[along]
    return tuple(gathered)


def in_blocks(shard, dim, length):
    lengths = shard.shape
    blocks = shard.reshape(*lengths[:dim], length, lengths[dim] // length, *lengths[dim + 1 :])
    return jnp.moveaxis(blocks, dim, 0)


def summed_on_arrival(shard, axis, dim):
    length = lax.axis_size(axis)
    blocks = lax.all_to_all(in_blocks(shard, dim, length), axis, 0, 0, tiled=True)
    return jnp.sum(blocks, axis=0)


def first_slots(needed, slots):
    running = jnp.cumsum(needed, axis=1) - 1
    levels = jnp.arange(slots, dtype=jnp.int32)[None, :, None]
    matches = (needed[:, None, :] == 1) & (running[:, None, :] == levels)
    places = jnp.arange(needed.shape[1], dtype=jnp.int32)[None, None, :]
    present = jnp.sum(matches.astype(jnp.int32), axis=2)
    located = jnp.sum(jnp.where(matches, places, 0), axis=2)
    return jnp.where(present > 0, located, -1)


def body(layer_input, queries, keys, values, outputs, d_out, log_sums, chosen):
    sequences, positions, channels = queries.shape
    head_count = log_sums.shape[2]
    head_size = channels // head_count
    local_blocks = positions // BLK
    devices = lax.axis_size("kv")
    my_index = lax.axis_index("kv")
    own_blocks = sequences * local_blocks
    inverse_root = head_size ** (-0.5)
    in_use = chosen >= 0
    owners = jnp.where(in_use, chosen // local_blocks, -1)
    remote = in_use & (owners != my_index)
    block_ids = jnp.arange(devices * local_blocks, dtype=jnp.int32)
    matched = (chosen[..., None] == block_ids) & remote[..., None]
    needed = jnp.max(matched.astype(jnp.int32), axis=(1, 2))
    needed = (
        needed.reshape(sequences, devices, local_blocks)
        .transpose(1, 0, 2)
        .reshape(devices, own_blocks)
    )
    everyone = over_pieces(needed, "kv")
    slot_table = first_slots(everyone, CAP)
    served = lax.dynamic_slice_in_dim(slot_table, my_index, 1, 0)
    key_rows = keys.reshape(own_blocks, BLK, channels)
    value_rows = values.reshape(own_blocks, BLK, channels)
    served_rows = jnp.maximum(served, 0).reshape(CAP)
    sent_keys = key_rows[served_rows]
    sent_values = value_rows[served_rows]
    got_keys, got_values = in_one_piece((sent_keys, sent_values), "kv", 0, 1)

    def head_major(rows, count):
        return rows.reshape(count, BLK, head_count, head_size).transpose(2, 0, 1, 3)

    pool_keys = jnp.concatenate(
        [head_major(key_rows, own_blocks), head_major(got_keys, devices * CAP)], axis=1
    )
    pool_values = jnp.concatenate(
        [head_major(value_rows, own_blocks), head_major(got_values, devices * CAP)], axis=1
    )
    pool_size = pool_keys.shape[1]
    seq_base = jnp.arange(sequences, dtype=jnp.int32)[:, None, None] * local_blocks
    local_place = seq_base + jnp.where(in_use, chosen % local_blocks, 0)
    owner_safe = jnp.maximum(owners, 0)
    owner_rows = slot_table[owner_safe]
    slot_match = owner_rows == local_place[..., None]
    slot_number = jnp.sum(jnp.where(slot_match, jnp.arange(CAP, dtype=jnp.int32), 0), axis=3)
    remote_place = own_blocks + owner_safe * CAP + slot_number
    pool_index = jnp.where(remote, remote_place, jnp.where(in_use, local_place, 0))

    def split_heads(rows):
        return rows.reshape(sequences, local_blocks, BLK, head_count, head_size).transpose(
            0, 3, 1, 2, 4
        )

    product = d_out.astype(jnp.float32) * outputs.astype(jnp.float32)
    deltas = jnp.sum(split_heads(product), axis=4)
    query_split = split_heads(queries)
    grad_split = split_heads(d_out)
    log_split = log_sums.reshape(sequences, local_blocks, BLK, head_count).transpose(0, 3, 1, 2)
    offsets = jnp.arange(BLK, dtype=jnp.int32)
    query_place = (my_index * local_blocks + jnp.arange(local_blocks, dtype=jnp.int32))[
        :, None
    ] * BLK + offsets[None, :]

    def advance(totals, bundle):
        key_total, value_total = totals
        query_rows, grad_rows, log_rows, delta_rows, index_rows, use_rows, chosen_rows = bundle
        key_picked = pool_keys[:, index_rows].reshape(
            head_count, local_blocks, SEL * BLK, head_size
        )
        value_picked = pool_values[:, index_rows].reshape(
            head_count, local_blocks, SEL * BLK, head_size
        )
        key_place = (jnp.maximum(chosen_rows, 0)[..., None] * BLK + offsets).reshape(
            local_blocks, SEL * BLK
        )
        key_live = jnp.broadcast_to(use_rows[..., None], (local_blocks, SEL, BLK)).reshape(
            local_blocks, SEL * BLK
        )
        visible = key_live[:, None, :] & (key_place[:, None, :] <= query_place[:, :, None])
        scores = (
            jnp.einsum(
                "hbqd,hbkd->hbqk", query_rows, key_picked, preferred_element_type=jnp.float32
            )
            * inverse_root
        )
        prob_full = jnp.where(visible[None], jnp.exp(scores - log_rows[..., None]), 0.0)
        prob_grad = jnp.einsum(
            "hbqd,hbkd->hbqk", grad_rows, value_picked, preferred_element_type=jnp.float32
        )
        score_grad = prob_full * (prob_grad - delta_rows[..., None])
        prob_low = prob_full.astype(jnp.bfloat16)
        score_low = score_grad.astype(jnp.bfloat16)
        grad_query = (
            jnp.einsum("hbqk,hbkd->hbqd", score_low, key_picked, preferred_element_type=jnp.float32)
            * inverse_root
        )
        grad_key = (
            jnp.einsum("hbqk,hbqd->hbkd", score_low, query_rows, preferred_element_type=jnp.float32)
            * inverse_root
        )
        grad_value = jnp.einsum(
            "hbqk,hbqd->hbkd", prob_low, grad_rows, preferred_element_type=jnp.float32
        )
        weight = use_rows.astype(jnp.float32).reshape(1, local_blocks * SEL, 1, 1)
        flat_index = index_rows.reshape(local_blocks * SEL)
        key_total = key_total.at[:, flat_index].add(
            grad_key.reshape(head_count, local_blocks * SEL, BLK, head_size) * weight
        )
        value_total = value_total.at[:, flat_index].add(
            grad_value.reshape(head_count, local_blocks * SEL, BLK, head_size) * weight
        )
        return ((key_total, value_total), grad_query.astype(jnp.bfloat16))

    zeroed = jnp.zeros((head_count, pool_size, BLK, head_size), jnp.float32)
    totals, query_grads = lax.scan(
        advance,
        (zeroed, zeroed),
        (query_split, grad_split, log_split, deltas, pool_index, in_use, chosen),
    )
    key_total, value_total = totals
    d_queries = query_grads.transpose(0, 2, 3, 1, 4).reshape(sequences, positions, channels)
    local_keys = key_total[:, :own_blocks]
    local_values = value_total[:, :own_blocks]
    remote_keys = key_total[:, own_blocks:]
    remote_values = value_total[:, own_blocks:]
    back_keys, back_values = (
        lax.psum_scatter(remote_keys, "kv", scatter_dimension=1, tiled=True),
        lax.psum_scatter(remote_values, "kv", scatter_dimension=1, tiled=True),
    )
    targets = jnp.where(served >= 0, served, own_blocks).reshape(CAP)
    local_keys = local_keys.at[:, targets].add(back_keys, mode="drop")
    local_values = local_values.at[:, targets].add(back_values, mode="drop")

    def token_major(total):
        low = total.astype(jnp.bfloat16).reshape(
            head_count, sequences, local_blocks, BLK, head_size
        )
        return low.transpose(1, 2, 3, 0, 4).reshape(sequences, positions, channels)

    d_keys = token_major(local_keys)
    d_values = token_major(local_values)
    whole_input = lax.all_gather(layer_input, "tp", axis=2, tiled=True)
    input_rows = whole_input.reshape(sequences * positions, whole_input.shape[2])
    value_grad_rows = d_values.reshape(sequences * positions, channels)
    d_weight = summed_on_arrival(
        lax.dot_general(
            input_rows,
            value_grad_rows,
            (((0,), (0,)), ((), ())),
            preferred_element_type=jnp.float32,
        ),
        "kv",
        0,
    )
    return (d_queries, d_keys, d_values, d_weight)


def solution(mesh):
    placed = (
        P(None, "kv", "tp"),
        P(None, "kv", "tp"),
        P(None, "kv", "tp"),
        P(None, "kv", "tp"),
        P(None, "kv", "tp"),
        P(None, "kv", "tp"),
        P(None, "kv", "tp"),
        P(None, "kv", None),
    )
    return jax.shard_map(
        body,
        mesh=mesh,
        in_specs=placed,
        out_specs=(P(None, "kv", "tp"), P(None, "kv", "tp"), P(None, "kv", "tp"), P("kv", "tp")),
        check_vma=False,
    )
```

profile of v0, /device:TPU:0, one launch (start us, length us, event | category | flops | bytes accessed | tf_op | source)
XLA Modules:
  0.0 925.2 jit_solution(1347397751227389841)
XLA Ops:
  10.3 26.4 %all_gather.9 = s32[32,32,32]{2,1,0:T(8,128)S(1)} all-gather(s32[1,32,32]{2,1,0:T(8,128)S(1)} %copy.65), channel_id=1, replica_groups=mesh['kv'=32,'tp'=4] {'kv'}, dimensions={0}, use_global_device_ids=true | all-gather | bytes 135168 | tf_op jit(solution)/shard_map/all_gather | solution.py:12
  73.3 22.1 %all-gather.3.cloned.1.call-done = bf16[64,128,512]{2,1,0:T(8,128)(2,1)} async-done(((bf16[2,128,512]{2,1,0:T(8,128)(2,1)}), bf16[64,128,512]{2,1,0:T(8,128)(2,1)}) %all-gather.3.cloned.1.call-update) | async-done | bytes 8388624 | tf_op jit(solution)/shard_map/all_gather | solution.py:18
  108.3 9.6 %pad_maximum_fusion.1 = bf16[4,96,64,128]{3,0,2,1:T(4,128)(2,1)} fusion(bf16[4,64,64,128]{3,0,2,1:T(4,128)(2,1)} %bitcast.142, bf16[4,32,64,128]{3,0,2,1:T(4,128)(2,1)} %bitcast.153), kind=kLoop, calls=%fused_computation.49 | loop fusion | flops 3145728 | bytes 12582912 | tf_op jit(solution)/shard_map/concatenate | solution.py:83
  132.1 9.6 %pad_maximum_fusion = bf16[4,96,64,128]{3,0,2,1:T(4,128)(2,1)} fusion(bf16[4,64,64,128]{3,0,2,1:T(4,128)(2,1)} %bitcast.143, bf16[4,32,64,128]{3,0,2,1:T(4,128)(2,1)} %bitcast.152), kind=kLoop, calls=%fused_computation.48 | loop fusion | flops 3145728 | bytes 12582912 | tf_op jit(solution)/shard_map/concatenate | solution.py:80
  161.0 499.8 %while.15 = (s32[]{:T(128)}, f32[4,96,64,128]{3,2,1,0:T(8,128)}, f32[4,96,64,128]{3,2,1,0:T(8,128)}, bf16[4,4,8,64,128]{4,3,2,1,0:T(8,128)(2,1)}, s32[4,8,12]{2,...) while((s32[]{:T(128)}, f32[4,96,64,128]{3,2,1,0:T(8,128)}, ...), condition=%wide.region_10.11_spmd.clone, body=%wide.region_7.10_spmd.clone.sunk | while | flops 2046042496 | bytes 275915360 | solution.py:162
  178.2 8.7 gather_fusion.1
  194.6 8.7 gather_fusion
  226.6 13.5 %fusion.60 = (f32[96,4,64,128]{3,2,1,0:T(8,128)}, f32[96,4,64,128]{3,2,1,0:T(8,128)}) fusion(f32[4,96,64,128]{3,2,1,0:T(8,128)} %bitcast.138, f32[96]{0:T(128)S(1)} %reshape.395, f32[4,96,64,128]{3,2,1,0:T(8,128)S(1)} %bitcast.135), kind=kLoop, calls=%fused_computation.12.clone.1 | loop fusion | flops 6291456 | bytes 50332032 | tf_op jit(solution)/shard_map/while/body/eval_jaxpr/mul | solution.py:157
  240.0 27.4 %scatter_fusion = f32[4,96,64,128]{3,2,1,0:T(8,128)} fusion(f32[4,96,64,128]{3,2,1,0:T(8,128)} %get-tuple-element.331, s32[96]{0:T(128)S(1)} %fusion.57, f32[96,4,64,128]{3,2,1,0:T(8,128)} %get-tuple-element.313), kind=kCustom, calls=%fused_computation.5.clone.clone.1 | custom fusion | flops 3145728 | bytes 37749120 | tf_op jit(solution)/shard_map/while/body/eval_jaxpr/scatter-add | solution.py:153
  267.4 28.4 %scatter_fusion.1 = f32[4,96,64,128]{3,2,1,0:T(8,128)} fusion(f32[4,96,64,128]{3,2,1,0:T(8,128)} %get-tuple-element.332, s32[96]{0:T(128)S(1)} %fusion.57, f32[96,4,64,128]{3,2,1,0:T(8,128)} %get-tuple-element.314), kind=kCustom, calls=%fused_computation.6.clone.clone.1 | custom fusion | flops 3145728 | bytes 37749120 | tf_op jit(solution)/shard_map/while/body/eval_jaxpr/scatter-add | solution.py:156
  300.1 8.7 gather_fusion.1
  316.5 8.7 gather_fusion
  348.5 13.5 %fusion.60 = (f32[96,4,64,128]{3,2,1,0:T(8,128)}, f32[96,4,64,128]{3,2,1,0:T(8,128)}) fusion(f32[4,96,64,128]{3,2,1,0:T(8,128)} %bitcast.138, f32[96]{0:T(128)S(1)} %reshape.395, f32[4,96,64,128]{3,2,1,0:T(8,128)S(1)} %bitcast.135), kind=kLoop, calls=%fused_computation.12.clone.1 | loop fusion | flops 6291456 | bytes 50332032 | tf_op jit(solution)/shard_map/while/body/eval_jaxpr/mul | solution.py:157
  361.9 27.5 %scatter_fusion = f32[4,96,64,128]{3,2,1,0:T(8,128)} fusion(f32[4,96,64,128]{3,2,1,0:T(8,128)} %get-tuple-element.331, s32[96]{0:T(128)S(1)} %fusion.57, f32[96,4,64,128]{3,2,1,0:T(8,128)} %get-tuple-element.313), kind=kCustom, calls=%fused_computation.5.clone.clone.1 | custom fusion | flops 3145728 | bytes 37749120 | tf_op jit(solution)/shard_map/while/body/eval_jaxpr/scatter-add | solution.py:153
  389.4 27.9 %scatter_fusion.1 = f32[4,96,64,128]{3,2,1,0:T(8,128)} fusion(f32[4,96,64,128]{3,2,1,0:T(8,128)} %get-tuple-element.332, s32[96]{0:T(128)S(1)} %fusion.57, f32[96,4,64,128]{3,2,1,0:T(8,128)} %get-tuple-element.314), kind=kCustom, calls=%fused_computation.6.clone.clone.1 | custom fusion | flops 3145728 | bytes 37749120 | tf_op jit(solution)/shard_map/while/body/eval_jaxpr/scatter-add | solution.py:156
  421.6 8.7 gather_fusion.1
  438.0 8.7 gather_fusion
  469.9 13.5 %fusion.60 = (f32[96,4,64,128]{3,2,1,0:T(8,128)}, f32[96,4,64,128]{3,2,1,0:T(8,128)}) fusion(f32[4,96,64,128]{3,2,1,0:T(8,128)} %bitcast.138, f32[96]{0:T(128)S(1)} %reshape.395, f32[4,96,64,128]{3,2,1,0:T(8,128)S(1)} %bitcast.135), kind=kLoop, calls=%fused_computation.12.clone.1 | loop fusion | flops 6291456 | bytes 50332032 | tf_op jit(solution)/shard_map/while/body/eval_jaxpr/mul | solution.py:157
  483.4 27.3 %scatter_fusion = f32[4,96,64,128]{3,2,1,0:T(8,128)} fusion(f32[4,96,64,128]{3,2,1,0:T(8,128)} %get-tuple-element.331, s32[96]{0:T(128)S(1)} %fusion.57, f32[96,4,64,128]{3,2,1,0:T(8,128)} %get-tuple-element.313), kind=kCustom, calls=%fused_computation.5.clone.clone.1 | custom fusion | flops 3145728 | bytes 37749120 | tf_op jit(solution)/shard_map/while/body/eval_jaxpr/scatter-add | solution.py:153
  510.8 28.0 %scatter_fusion.1 = f32[4,96,64,128]{3,2,1,0:T(8,128)} fusion(f32[4,96,64,128]{3,2,1,0:T(8,128)} %get-tuple-element.332, s32[96]{0:T(128)S(1)} %fusion.57, f32[96,4,64,128]{3,2,1,0:T(8,128)} %get-tuple-element.314), kind=kCustom, calls=%fused_computation.6.clone.clone.1 | custom fusion | flops 3145728 | bytes 37749120 | tf_op jit(solution)/shard_map/while/body/eval_jaxpr/scatter-add | solution.py:156
  543.0 8.7 gather_fusion.1
  559.4 8.7 gather_fusion
  591.4 13.5 %fusion.60 = (f32[96,4,64,128]{3,2,1,0:T(8,128)}, f32[96,4,64,128]{3,2,1,0:T(8,128)}) fusion(f32[4,96,64,128]{3,2,1,0:T(8,128)} %bitcast.138, f32[96]{0:T(128)S(1)} %reshape.395, f32[4,96,64,128]{3,2,1,0:T(8,128)S(1)} %bitcast.135), kind=kLoop, calls=%fused_computation.12.clone.1 | loop fusion | flops 6291456 | bytes 50332032 | tf_op jit(solution)/shard_map/while/body/eval_jaxpr/mul | solution.py:157
  604.8 27.3 %scatter_fusion = f32[4,96,64,128]{3,2,1,0:T(8,128)} fusion(f32[4,96,64,128]{3,2,1,0:T(8,128)} %get-tuple-element.331, s32[96]{0:T(128)S(1)} %fusion.57, f32[96,4,64,128]{3,2,1,0:T(8,128)} %get-tuple-element.313), kind=kCustom, calls=%fused_computation.5.clone.clone.1 | custom fusion | flops 3145728 | bytes 37749120 | tf_op jit(solution)/shard_map/while/body/eval_jaxpr/scatter-add | solution.py:153
  632.1 28.4 %scatter_fusion.1 = f32[4,96,64,128]{3,2,1,0:T(8,128)} fusion(f32[4,96,64,128]{3,2,1,0:T(8,128)} %get-tuple-element.332, s32[96]{0:T(128)S(1)} %fusion.57, f32[96,4,64,128]{3,2,1,0:T(8,128)} %get-tuple-element.314), kind=kCustom, calls=%fused_computation.6.clone.clone.1 | custom fusion | flops 3145728 | bytes 37749120 | tf_op jit(solution)/shard_map/while/body/eval_jaxpr/scatter-add | solution.py:156
  660.8 11.9 %copy.80 = f32[4,96,64,128]{3,2,0,1:T(8,128)} copy(f32[4,96,64,128]{3,2,1,0:T(8,128)} %get-tuple-element.85) | data formatting | bytes 25165824 | tf_op jit(solution)/shard_map/while | solution.py:162
  672.7 8.3 slice.37
  681.6 11.9 %copy.78 = f32[4,96,64,128]{3,2,0,1:T(8,128)} copy(f32[4,96,64,128]{3,2,1,0:T(8,128)} %get-tuple-element.84) | data formatting | bytes 25165824 | tf_op jit(solution)/shard_map/while | solution.py:162
  693.5 10.0 %slice.36 = f32[4,64,64,128]{3,2,0,1:T(8,128)} slice(f32[4,96,64,128]{3,2,0,1:T(8,128)} %copy.78), slice={[0:4], [32:96], [0:64], [0:128]} | slice | bytes 16777216 | tf_op jit(solution)/shard_map/slice | solution.py:171
  708.9 73.1 %reduce-scatter.5.cloned.1.call-done = f32[4,2,64,128]{3,2,0,1:T(8,128)} async-done(((f32[4,64,64,128]{3,2,0,1:T(8,128)}), f32[4,2,64,128]{3,2,0,1:T(8,128)}) %reduce-scatter.5.cloned.1.call-update) | async-done | bytes 262160 | tf_op jit(solution)/shard_map/reduce_scatter | solution.py:175
  789.1 9.5 %convolution_bitcast_fusion = f32[2048,512]{0,1:T(8,128)} fusion(bf16[2048,2048]{1,0:T(8,128)(2,1)} %bitcast.163, bf16[256,8,4,128]{3,2,1,0:T(4,128)(2,1)S(1)} %bitcast.149), kind=kOutput, calls=%fused_computation.51 | convolution fusion | flops 4294967296 | bytes 14680064 | tf_op jit(solution)/shard_map/dot_general | solution.py:193
  822.3 77.5 %reduce-scatter.3.cloned.1.call-done = f32[4,2,64,128]{3,2,0,1:T(8,128)} async-done(((f32[4,64,64,128]{3,2,0,1:T(8,128)}), f32[4,2,64,128]{3,2,0,1:T(8,128)}) %reduce-scatter.3.cloned.1.call-update) | async-done | bytes 262160 | tf_op jit(solution)/shard_map/reduce_scatter | solution.py:174
  (252 shorter events, 280.1 us)
Async XLA Ops:
  8.0 41.4 %copy-start.6 = (s32[4,8,12]{2,1,0:T(8,128)S(1)}, s32[4,8,12]{2,1,0:T(8,128)}, u32[]{:S(2)}) copy-start(s32[4,8,12]{2,1,0:T(8,128)} %param.17) | copy-start | bytes 4612
  8.0 39.3 %copy-start.4 = (bf16[4,512,512]{2,1,0:T(8,128)(2,1)S(1)}, bf16[4,512,512]{2,1,0:T(8,128)(2,1)}, u32[]{:S(2)}) copy-start(bf16[4,512,512]{2,1,0:T(8,128)(2,1)} %param.13) | copy-start | bytes 6291460
  8.0 41.5 %copy-start.11 = (f32[4,512,4]{1,2,0:T(4,128)S(1)}, f32[4,512,4]{1,2,0:T(4,128)}, u32[]{:S(2)}) copy-start(f32[4,512,4]{1,2,0:T(4,128)} %param.16) | copy-start | bytes 98308
  8.0 87.3 %all-gather.3.cloned.1.call-start = ((), (), s32[]{:S(2)}) async-start(), calls=%async_computation.3 | async-start | bytes 8650752 | tf_op jit(solution)/shard_map/all_gather | solution.py:18
  43.1 738.9 %reduce-scatter.5.cloned.1.call-start = ((), (), s32[]{:S(2)}) async-start(), calls=%async_computation.5 | async-start | bytes 8650752 | tf_op jit(solution)/shard_map/reduce_scatter | solution.py:175
  174.0 12.9 %copy-start.2 = (bf16[4,4,8,64,128]{4,1,3,2,0:T(4,128)(2,1)}, bf16[4,4,8,64,128]{4,1,3,2,0:T(4,128)(2,1)S(1)}, u32[]{:S(2)}) copy-start(bf16[4,4,8,64,128]{4,1,3,2,0:T(4,128)(2,1)S(1)} %get-tuple-element.352) | copy-start | bytes 6291460 | tf_op jit(solution)/shard_map/while
  203.3 4.3 copy-start
  215.4 2.1 copy-start.1
  267.4 28.4 %copy-start.3 = (bf16[4,4,8,64,128]{4,1,3,2,0:T(4,128)(2,1)S(1)}, bf16[4,4,8,64,128]{4,1,3,2,0:T(4,128)(2,1)}, u32[]{:S(2)}) copy-start(bf16[4,4,8,64,128]{4,1,3,2,0:T(4,128)(2,1)} %copy-done.2) | copy-start | bytes 6291460 | tf_op jit(solution)/shard_map/while
  267.4 28.4 %copy-start.8 = (f32[4,4,8,64]{3,2,1,0:T(8,128)S(1)}, f32[4,4,8,64]{3,2,1,0:T(8,128)}, u32[]{:S(2)}) copy-start(f32[4,4,8,64]{3,2,1,0:T(8,128)} %copy-done.7) | copy-start | bytes 98308 | tf_op jit(solution)/shard_map/while
  267.4 28.4 %copy-start.10 = (s32[4,8,12]{2,1,0:T(8,128)S(1)}, s32[4,8,12]{2,1,0:T(8,128)}, u32[]{:S(2)}) copy-start(s32[4,8,12]{2,1,0:T(8,128)} %copy-done.9) | copy-start | bytes 4612 | tf_op jit(solution)/shard_map/while
  295.9 12.9 %copy-start.2 = (bf16[4,4,8,64,128]{4,1,3,2,0:T(4,128)(2,1)}, bf16[4,4,8,64,128]{4,1,3,2,0:T(4,128)(2,1)S(1)}, u32[]{:S(2)}) copy-start(bf16[4,4,8,64,128]{4,1,3,2,0:T(4,128)(2,1)S(1)} %get-tuple-element.352) | copy-start | bytes 6291460 | tf_op jit(solution)/shard_map/while
  325.2 4.3 copy-start
  389.4 27.9 %copy-start.3 = (bf16[4,4,8,64,128]{4,1,3,2,0:T(4,128)(2,1)S(1)}, bf16[4,4,8,64,128]{4,1,3,2,0:T(4,128)(2,1)}, u32[]{:S(2)}) copy-start(bf16[4,4,8,64,128]{4,1,3,2,0:T(4,128)(2,1)} %copy-done.2) | copy-start | bytes 6291460 | tf_op jit(solution)/shard_map/while
  389.4 27.9 %copy-start.8 = (f32[4,4,8,64]{3,2,1,0:T(8,128)S(1)}, f32[4,4,8,64]{3,2,1,0:T(8,128)}, u32[]{:S(2)}) copy-start(f32[4,4,8,64]{3,2,1,0:T(8,128)} %copy-done.7) | copy-start | bytes 98308 | tf_op jit(solution)/shard_map/while
  389.4 27.9 %copy-start.10 = (s32[4,8,12]{2,1,0:T(8,128)S(1)}, s32[4,8,12]{2,1,0:T(8,128)}, u32[]{:S(2)}) copy-start(s32[4,8,12]{2,1,0:T(8,128)} %copy-done.9) | copy-start | bytes 4612 | tf_op jit(solution)/shard_map/while
  417.4 12.9 %copy-start.2 = (bf16[4,4,8,64,128]{4,1,3,2,0:T(4,128)(2,1)}, bf16[4,4,8,64,128]{4,1,3,2,0:T(4,128)(2,1)S(1)}, u32[]{:S(2)}) copy-start(bf16[4,4,8,64,128]{4,1,3,2,0:T(4,128)(2,1)S(1)} %get-tuple-element.352) | copy-start | bytes 6291460 | tf_op jit(solution)/shard_map/while
  446.6 4.3 copy-start
  458.8 2.1 copy-start.1
  510.7 28.0 %copy-start.3 = (bf16[4,4,8,64,128]{4,1,3,2,0:T(4,128)(2,1)S(1)}, bf16[4,4,8,64,128]{4,1,3,2,0:T(4,128)(2,1)}, u32[]{:S(2)}) copy-start(bf16[4,4,8,64,128]{4,1,3,2,0:T(4,128)(2,1)} %copy-done.2) | copy-start | bytes 6291460 | tf_op jit(solution)/shard_map/while
  510.7 28.0 %copy-start.8 = (f32[4,4,8,64]{3,2,1,0:T(8,128)S(1)}, f32[4,4,8,64]{3,2,1,0:T(8,128)}, u32[]{:S(2)}) copy-start(f32[4,4,8,64]{3,2,1,0:T(8,128)} %copy-done.7) | copy-start | bytes 98308 | tf_op jit(solution)/shard_map/while
  510.7 28.0 %copy-start.10 = (s32[4,8,12]{2,1,0:T(8,128)S(1)}, s32[4,8,12]{2,1,0:T(8,128)}, u32[]{:S(2)}) copy-start(s32[4,8,12]{2,1,0:T(8,128)} %copy-done.9) | copy-start | bytes 4612 | tf_op jit(solution)/shard_map/while
  538.8 12.9 %copy-start.2 = (bf16[4,4,8,64,128]{4,1,3,2,0:T(4,128)(2,1)}, bf16[4,4,8,64,128]{4,1,3,2,0:T(4,128)(2,1)S(1)}, u32[]{:S(2)}) copy-start(bf16[4,4,8,64,128]{4,1,3,2,0:T(4,128)(2,1)S(1)} %get-tuple-element.352) | copy-start | bytes 6291460 | tf_op jit(solution)/shard_map/while
  568.1 4.3 copy-start
  632.1 28.4 %copy-start.3 = (bf16[4,4,8,64,128]{4,1,3,2,0:T(4,128)(2,1)S(1)}, bf16[4,4,8,64,128]{4,1,3,2,0:T(4,128)(2,1)}, u32[]{:S(2)}) copy-start(bf16[4,4,8,64,128]{4,1,3,2,0:T(4,128)(2,1)} %copy-done.2) | copy-start | bytes 6291460 | tf_op jit(solution)/shard_map/while
  632.1 28.4 %copy-start.8 = (f32[4,4,8,64]{3,2,1,0:T(8,128)S(1)}, f32[4,4,8,64]{3,2,1,0:T(8,128)}, u32[]{:S(2)}) copy-start(f32[4,4,8,64]{3,2,1,0:T(8,128)} %copy-done.7) | copy-start | bytes 98308 | tf_op jit(solution)/shard_map/while
  632.1 28.4 %copy-start.10 = (s32[4,8,12]{2,1,0:T(8,128)S(1)}, s32[4,8,12]{2,1,0:T(8,128)}, u32[]{:S(2)}) copy-start(s32[4,8,12]{2,1,0:T(8,128)} %copy-done.9) | copy-start | bytes 4612 | tf_op jit(solution)/shard_map/while
  681.0 108.1 %all-gather.5.cloned.1.call-start = ((), (), s32[]{:S(2)}) async-start(), calls=%async_computation.6 | async-start | bytes 10485760 | tf_op jit(solution)/shard_map/all_gather | solution.py:189
  681.6 218.2 %reduce-scatter.3.cloned.1.call-start = ((), (), s32[]{:S(2)}) async-start(), calls=%async_computation.4 | async-start | bytes 8650752 | tf_op jit(solution)/shard_map/reduce_scatter | solution.py:174
  703.5 78.5 %copy-start.12 = (s32[2]{0:T(128)S(1)}, s32[2]{0:T(128)}, u32[]{:S(2)}) copy-start(s32[2]{0:T(128)} %get-tuple-element.204) | copy-start | bytes 28
  804.1 110.3 %all-to-all-start = ((f32[32,64,512]{2,1,0:T(8,128)}), f32[32,64,512]{2,1,0:T(8,128)}, u32[]{:S(2)}, u32[]{:S(2)}) async-start(f32[32,64,512]{2,1,0:T(8,128)} %bitcast.144), calls=%async_computation.2 | async-start | bytes 8388608 | tf_op jit(solution)/shard_map/all_to_all | solution.py:33
  809.7 5.1 copy-start.5
  (10 other events, 14.8 us)
Sparse Core Ops, SparseCore 0:
  43.2 52.1 all-gather.2
  681.1 100.8 reduce-scatter.4
  785.7 114.0 reduce-scatter.2
Sparse Core Ops, SparseCore 1:
  683.1 90.8 all-gather.4
where the time goes:
time: 931 us; the launch traced here: 925 us
  other arithmetic  326 us (35%)
  local copies, waits for them, and re-layouts  279 us (30%)
  waiting for transfers between devices  173 us (19%)
  matrix products  85.1 us (9%)
  blocking collectives  26.4 us (3%)
  between operations  15.8 us (2%)
  loops' own time  13.7 us (1%)
    scatter-add x4, other arithmetic, advance(): value_total.at[:, flat_index]  113 us
    scatter-add x4, other arithmetic, advance(): key_total.at[:, flat_index]  110 us
    reduce_scatter x1, waiting for transfers between devices, body(): lax.psum_scatter(remote_keys, 'kv', scatter_dimension=1, tiled=True)  77.5 us
    reduce_scatter x1, waiting for transfers between devices, body(): lax.psum_scatter(remote_values, 'kv', scatter_dimension=1, tiled=True)  73.1 us
    gather x8, local copies, waits for them, and re-layouts, advance(): pool_values[:, index_rows]  65.4 us
    mul x4, other arithmetic, advance(): grad_value.reshape(head_count, local_blocks * SEL, BLK, head_size) * weight  53.9 us
    gather x8, local copies, waits for them, and re-layouts, advance(): pool_keys[:, index_rows]  52.2 us
    all_gather x1, blocking collectives, over_pieces(): blocks = lax.all_gather(shard, axis)  26.4 us
  transfers between devices with their start and end apart: 5, of which 3 were waited for; matrix products, arithmetic and copies ran while one was open for 12% of the time, Pallas kernels for 0%

commit v1 on v0

v1 whole, which is shorter than its diff:
```python
import functools
import jax
import jax.numpy as jnp
from jax import lax
from jax.experimental import pallas as pl
from jax.experimental.pallas import tpu as pltpu
from jax.sharding import PartitionSpec as P

BLK = 64
CAP = 2
DH = 128
LOG2E = 1.4426950408889634
ROOT = DH ** -0.5
BIG = 1e30

NT = (((1,), (1,)), ((), ()))
TN = (((0,), (0,)), ((), ()))
NN = (((1,), (0,)), ((), ()))


def mm(a, b, dims):
    return lax.dot_general(a, b, dims, preferred_element_type=jnp.float32)


def local_kernel(q_ref, k_ref, v_ref, o_ref, do_ref, lse_ref, sel_ref,
                 dqt_ref, dk_ref, dv_ref, delta_ref):
    heads = q_ref.shape[2] // DH
    n = q_ref.shape[1]
    half = n // 2
    for h in range(heads):
        hs = slice(h * DH, (h + 1) * DH)
        q = q_ref[0, :, hs]
        do = do_ref[0, :, hs]
        prod = do.astype(jnp.float32) * o_ref[0, :, hs].astype(jnp.float32)
        delta = jnp.sum(prod.T, axis=0, keepdims=True)
        delta_ref[0, h:h + 1, :] = delta
        lse = lse_ref[0, h:h + 1, :]
        parts = []
        for c in range(2):
            lo = c * half
            k = k_ref[0, lo:lo + half, hs]
            v = v_ref[0, lo:lo + half, hs]
            qc = q[lo:]
            doc = do[lo:]
            w = n - lo
            s = mm(k, qc, NT)
            row = lax.broadcasted_iota(jnp.int32, (half, w), 0)
            col = lax.broadcasted_iota(jnp.int32, (half, w), 1)
            bias = jnp.concatenate(
                [jnp.broadcast_to(lse[:, lo:] + sel_ref[0, j:j + 1, lo:], (BLK, w))
                 for j in range(lo // BLK, (lo + half) // BLK)], axis=0)
            x = jnp.where(row <= col, s * (ROOT * LOG2E) - bias, -BIG)
            p = jnp.exp2(x)
            dp = mm(v, doc, NT)
            ds = (p * (dp - delta[:, lo:])).astype(jnp.bfloat16)
            dv_ref[0, lo:lo + half, hs] = mm(p.astype(jnp.bfloat16), doc, NN).astype(jnp.bfloat16)
            dk_ref[0, lo:lo + half, hs] = (mm(ds, qc, NN) * ROOT).astype(jnp.bfloat16)
            parts.append(mm(k, ds, TN))
        dqt_ref[0, hs, :half] = parts[0][:, :half]
        dqt_ref[0, hs, half:] = parts[0][:, half:] + parts[1]


def remote_kernel(seq_ref, q_ref, do_ref, lse_ref, delta_ref, sel_ref, pk_ref, pv_ref, dqt_in,
                  dq_ref, gk_ref, gv_ref, acc, list_ref, cnt_ref):
    seqs = 4
    heads = q_ref.shape[2] // DH
    slots = pk_ref.shape[0]
    s = pl.program_id(0)

    @pl.when(s == 0)
    def _():
        for t in range(seqs):
            cnt_ref[t] = 0

        def scan(i, _):
            t = seq_ref[i]

            @pl.when(t >= 0)
            def _():
                c = cnt_ref[t]
                list_ref[t, c] = i
                cnt_ref[t] = c + 1

            @pl.when(t < 0)
            def _():
                gk_ref[i] = jnp.zeros(gk_ref.shape[1:], gk_ref.dtype)
                gv_ref[i] = jnp.zeros(gv_ref.shape[1:], gv_ref.dtype)
            return 0

        lax.fori_loop(0, slots, scan, 0)

    acc[...] = dqt_in[0]
    n = cnt_ref[s]

    def chunk(c, _):
        ids = []
        for e in range(4):
            at = c * 4 + e
            i = list_ref[s, jnp.minimum(at, n - 1)]
            ids.append((i, jnp.where(at < n, i, slots)))
        for h in range(heads):
            hs = slice(h * DH, (h + 1) * DH)
            q = q_ref[0, :, hs]
            do = do_ref[0, :, hs]
            k = jnp.concatenate([pk_ref[i, :, hs] for i, _ in ids], axis=0)
            v = jnp.concatenate([pv_ref[i, :, hs] for i, _ in ids], axis=0)
            lse = lse_ref[0, h:h + 1, :]
            st = mm(k, q, NT)
            bias = jnp.concatenate(
                [jnp.broadcast_to(lse + sel_ref[j], (BLK, lse.shape[1])) for _, j in ids], axis=0)
            p = jnp.exp2(st * (ROOT * LOG2E) - bias)
            dp = mm(v, do, NT)
            ds = (p * (dp - delta_ref[0, h:h + 1, :])).astype(jnp.bfloat16)
            dv = mm(p.astype(jnp.bfloat16), do, NN).astype(jnp.bfloat16)
            dk = (mm(ds, q, NN) * ROOT).astype(jnp.bfloat16)
            for e, (_, j) in enumerate(ids):
                gv_ref[j, :, hs] = dv[e * BLK:(e + 1) * BLK]
                gk_ref[j, :, hs] = dk[e * BLK:(e + 1) * BLK]
            acc[hs, :] += mm(k, ds, TN)
        return 0

    lax.fori_loop(0, (n + 3) // 4, chunk, 0)
    for h in range(heads):
        hs = slice(h * DH, (h + 1) * DH)
        dq_ref[0, :, hs] = (acc[hs, :].T * ROOT).astype(jnp.bfloat16)


def local_attention(q, k, v, o, do, lse, sel):
    seqs, n, ch = q.shape
    heads = ch // DH
    big = pl.BlockSpec((1, n, ch), lambda s: (s, 0, 0))
    small = pl.BlockSpec((1, heads, n), lambda s: (s, 0, 0))
    return pl.pallas_call(
        local_kernel,
        grid=(seqs,),
        in_specs=[big] * 5 + [small, pl.BlockSpec((1, n // BLK, n), lambda s: (s, 0, 0))],
        out_specs=[pl.BlockSpec((1, ch, n), lambda s: (s, 0, 0)), big, big, small],
        out_shape=[
            jax.ShapeDtypeStruct((seqs, ch, n), jnp.float32),
            jax.ShapeDtypeStruct(q.shape, jnp.bfloat16),
            jax.ShapeDtypeStruct(q.shape, jnp.bfloat16),
            jax.ShapeDtypeStruct((seqs, heads, n), jnp.float32),
        ],
        compiler_params=pltpu.CompilerParams(vmem_limit_bytes=48 * 1024 * 1024),
        cost_estimate=pl.CostEstimate(flops=5 * 2 * seqs * heads * n * n * DH, bytes_accessed=22 << 20,
                                      transcendentals=seqs * heads * n * n),
        name="local_attention",
    )(q, k, v, o, do, lse, sel)


def remote_attention(slot_seq, q, do, lse, delta, sel, pk, pv, dqt):
    seqs, n, ch = q.shape
    heads = ch // DH
    slots = pk.shape[0]
    big = pl.BlockSpec((1, n, ch), lambda s: (s, 0, 0))
    small = pl.BlockSpec((1, heads, n), lambda s: (s, 0, 0))
    whole = pl.BlockSpec(memory_space=pltpu.VMEM)
    return pl.pallas_call(
        remote_kernel,
        grid=(seqs,),
        in_specs=[pl.BlockSpec(memory_space=pltpu.SMEM), big, big, small, small, whole, whole, whole,
                  pl.BlockSpec((1, ch, n), lambda s: (s, 0, 0))],
        out_specs=[big, whole, whole],
        out_shape=[
            jax.ShapeDtypeStruct(q.shape, jnp.bfloat16),
            jax.ShapeDtypeStruct((slots + 1, BLK, ch), jnp.bfloat16),
            jax.ShapeDtypeStruct((slots + 1, BLK, ch), jnp.bfloat16),
        ],
        scratch_shapes=[
            pltpu.VMEM((ch, n), jnp.float32),
            pltpu.SMEM((seqs, slots), jnp.int32),
            pltpu.SMEM((seqs,), jnp.int32),
        ],
        compiler_params=pltpu.CompilerParams(vmem_limit_bytes=60 * 1024 * 1024),
        cost_estimate=pl.CostEstimate(flops=5 * 2 * heads * slots * BLK * n * DH, bytes_accessed=28 << 20,
                                      transcendentals=heads * slots * BLK * n),
        name="remote_attention",
    )(slot_seq, q, do, lse, delta, sel, pk, pv, dqt)


def first_slots(needed, slots):
    running = jnp.cumsum(needed, axis=1) - 1
    levels = jnp.arange(slots, dtype=jnp.int32)[None, :, None]
    matches = (needed[:, None, :] == 1) & (running[:, None, :] == levels)
    places = jnp.arange(needed.shape[1], dtype=jnp.int32)[None, None, :]
    present = jnp.sum(matches.astype(jnp.int32), axis=2)
    located = jnp.sum(jnp.where(matches, places, 0), axis=2)
    return jnp.where(present > 0, located, -1)


def body(layer_input, queries, keys, values, outputs, d_out, log_sums, chosen):
    seqs, n, ch = queries.shape
    local_blocks = n // BLK
    devices = lax.axis_size("kv")
    me = lax.axis_index("kv")
    own = seqs * local_blocks
    lse = jnp.swapaxes(log_sums, 1, 2) * LOG2E

    in_use = chosen >= 0
    remote = in_use & (chosen // local_blocks != me)
    ids = jnp.arange(devices * local_blocks, dtype=jnp.int32)
    needed = jnp.max(((chosen[..., None] == ids) & remote[..., None]).astype(jnp.int32), axis=(1, 2))
    needed = needed.reshape(seqs, devices, local_blocks).transpose(1, 0, 2).reshape(devices, own)
    everyone = lax.all_gather(needed, "kv").max(axis=0)
    table = first_slots(everyone, CAP)
    served = lax.dynamic_slice_in_dim(table, me, 1, 0).reshape(CAP)
    rows = jnp.maximum(served, 0)
    sent = jnp.concatenate([keys.reshape(own, BLK, ch)[rows], values.reshape(own, BLK, ch)[rows]], axis=0)
    pool = lax.all_gather(sent, "kv", axis=0)
    pk = pool[:, :CAP].reshape(devices * CAP, BLK, ch)
    pv = pool[:, CAP:].reshape(devices * CAP, BLK, ch)

    mine = me * local_blocks + jnp.arange(local_blocks, dtype=jnp.int32)
    picked = jnp.any(chosen[:, None, :, :] == mine[None, :, None, None], axis=3)
    sel_local = jnp.repeat(jnp.where(picked, 0.0, BIG).astype(jnp.float32), BLK, axis=2)
    dqt, dk_local, dv_local, delta = local_attention(
        queries, keys, values, outputs, d_out, lse, sel_local)

    flat = table.reshape(devices * CAP)
    owner = jnp.arange(devices * CAP, dtype=jnp.int32) // CAP
    slot_seq = jnp.where(flat >= 0, flat // local_blocks, -1)
    slot_id = jnp.where(flat >= 0, owner * local_blocks + flat % local_blocks, -2)
    named = jnp.any(chosen[:, None] == slot_id[None, :, None, None], axis=3)
    named = named & (slot_seq[None, :, None] == jnp.arange(seqs, dtype=jnp.int32)[:, None, None])
    named = jnp.any(named, axis=0) & (owner != me)[:, None]
    slot_seq = jnp.where(jnp.any(named, axis=1), slot_seq, -1)
    sel_remote = jnp.repeat(jnp.where(named, 0.0, BIG).astype(jnp.float32), BLK, axis=1)
    sel_remote = jnp.concatenate([sel_remote, jnp.full((8, n), BIG, jnp.float32)], axis=0)[:, None, :]
    d_queries, gk, gv = remote_attention(slot_seq, queries, d_out, lse, delta, sel_remote, pk, pv, dqt)

    slots = devices * CAP
    back = jnp.concatenate(
        [gk[:slots].reshape(devices, CAP, BLK, ch), gv[:slots].reshape(devices, CAP, BLK, ch)], axis=1)
    back = lax.psum_scatter(back, "kv", scatter_dimension=0).astype(jnp.float32)
    hot = (served[:, None] == jnp.arange(own, dtype=jnp.int32)[None, :]).astype(jnp.float32)

    def finish(local, extra):
        full = local.reshape(own, BLK, ch).astype(jnp.float32)
        for c in range(CAP):
            full = full + hot[c][:, None, None] * extra[c][None]
        return full.astype(jnp.bfloat16).reshape(seqs, n, ch)

    d_keys = finish(dk_local, back[:CAP])
    d_values = finish(dv_local, back[CAP:])
    whole = lax.all_gather(layer_input, "tp", axis=2, tiled=True)
    d_weight = lax.dot_general(
        whole.reshape(seqs * n, whole.shape[2]), d_values.reshape(seqs * n, ch), TN,
        preferred_element_type=jnp.float32)
    d_weight = lax.psum_scatter(d_weight, "kv", scatter_dimension=0, tiled=True)
    return d_queries, d_keys, d_values, d_weight


def solution(mesh):
    spec = P(None, "kv", "tp")
    return jax.shard_map(
        body,
        mesh=mesh,
        in_specs=(spec,) * 7 + (P(None, "kv", None),),
        out_specs=(spec, spec, spec, P("kv", "tp")),
        check_vma=False,
    )
```

time: 931 us -> 353 us (0.38)
  other arithmetic: 326 us -> 15.3 us
  local copies, waits for them, and re-layouts: 279 us -> 30.7 us
  matrix products: 85.1 us -> 10.5 us
  waiting for transfers between devices: 173 us -> 230 us
  Pallas kernels: 0 us -> 24.5 us
  loops' own time: 13.7 us -> 0 us
    scatter-add x10 -> x0, other arithmetic: 227 us -> none  [the longest x4 113 us: advance(): value_total.at[:, flat_index]]
    gather x21 -> x2, local copies, waits for them, and re-layouts: 123 us -> 4.29 us  [the longest x1 2.15 us: body(): keys.reshape(own, BLK, ch)[rows]]
    unnamed x4 -> x5, waiting for transfers between devices: 0.57 us -> 82.4 us
    dot_general x21 -> x1, matrix products: 85.1 us -> 10.5 us  [body(): lax.dot_general(whole.reshape(seqs * n, whole.shape[2]), d_values.reshape...]
    mul x11 -> x1, other arithmetic: 59.3 us -> 0.01 us  [body(): lse = jnp.swapaxes(log_sums, 1, 2) * LOG2E]
    reshape x16 -> x3, local copies, waits for them, and re-layouts: 42.2 us -> 0.31 us  [the longest x1 0.12 us: body(): jnp.repeat(jnp.where(named, 0.0, BIG).astype(jnp.float32), BLK, axis=1)]
    reduce_scatter x2 -> x1, waiting for transfers between devices: 151 us -> 112 us  [body(): back = lax.psum_scatter(back, 'kv', scatter_dimension=0).astype(jnp.float32)]
    pallas_call x0 -> x2, Pallas kernels: none -> 24.5 us  [the longest x1 12.3 us: remote_attention(): pl.pallas_call(remote_kernel, grid=(seqs,), in_specs=[pl.BlockSpec(memory...]
  transfers between devices with their start and end apart: 5 -> 4, of which waited for: 3 -> 3; matrix products, arithmetic and copies ran while one was open for 12% -> 3% of each run, Pallas kernels for 0% -> 3%
where the time goes in v1:
time: 353 us
  waiting for transfers between devices  230 us (65%)
  local copies, waits for them, and re-layouts  30.7 us (9%)
  blocking collectives  26.4 us (7%)
  Pallas kernels  24.5 us (7%)
  between operations  15.4 us (4%)
  other arithmetic  15.3 us (4%)
  matrix products  10.5 us (3%)
    reduce_scatter x1, waiting for transfers between devices, body(): back = lax.psum_scatter(back, 'kv', scatter_dimension=0).astype(jnp.float32)  112 us
    unnamed x5, waiting for transfers between devices  82.4 us
    all_gather x1, waiting for transfers between devices, body(): pool = lax.all_gather(sent, 'kv', axis=0)  35.1 us
    all_gather x1, blocking collectives, body(): everyone = lax.all_gather(needed, 'kv').max(axis=0)  26.4 us
    pallas_call x1, Pallas kernels, remote_attention(): pl.pallas_call(remote_kernel, grid=(seqs,), in_specs=[pl.BlockSpec(memory...  12.3 us
    pallas_call x1, Pallas kernels, local_attention(): pl.pallas_call(local_kernel, grid=(seqs,), in_specs=[big] * 5 + [small, p...  12.2 us
    dot_general x1, matrix products, body(): lax.dot_general(whole.reshape(seqs * n, whole.shape[2]), d_values.reshape...  10.5 us
    unnamed x17, local copies, waits for them, and re-layouts  8.7 us
  transfers between devices with their start and end apart: 4, of which 3 were waited for; matrix products, arithmetic and copies ran while one was open for 3% of the time, Pallas kernels for 3%

profile of v1, /device:TPU:0, one launch (start us, length us, event | category | flops | bytes accessed | tf_op | source)
XLA Modules:
  0.0 352.9 jit_solution(4874960622841446035)
XLA Ops:
  8.1 0.8 copy.36
  8.9 0.7 compare_and_fusion
  9.7 0.2 convert_reduce_fusion
  10.2 26.4 %all_gather.12 = s32[32,32,32]{2,1,0:T(8,128)S(1)} all-gather(s32[1,32,32]{2,1,0:T(8,128)S(1)} %copy.40), channel_id=1, replica_groups=mesh['kv'=32,'tp'=4] {'kv'}, dimensions={0}, use_global_device_ids=true | all-gather | bytes 135168 | tf_op jit(solution)/shard_map/all_gather | solution.py:204
  37.4 2.1 gather_fusion
  39.5 2.1 gather_fusion.1
  41.7 0.7 pad_maximum_fusion.1
  43.2 0.8 broadcast_in_dim.78.sel_ref
  44.0 0.7 compare_reduce_fusion.1
  44.9 0.6 broadcast_select_fusion.1.seq_ref
  45.5 12.2 %local_attention.1 = (f32[4,512,512]{2,1,0:T(8,128)}, bf16[4,512,512]{2,1,0:T(8,128)(2,1)S(1)}, bf16[4,512,512]{2,1,0:T(8,128)(2,1)S(1)}, f32[4,4,512]{2,1,0:T(4,128)S(1)}) custom-call(bf16[4,512,512]{2,1,0:T(8,128)(2,1)} %q_ref.3, bf16[4,512,512]{2,1,0:T(8,128)(2,1)} %k_ref.1, bf16[4,512,512]{2,1,0:T(8,128)(2,1)} %v_ref.1, bf16[4,512,512]{2,1,0:T(8,128)(2,1)} %o_ref.1, ...), custom_call_target="tpu_custom_call" | custom-call | flops 5368709120 | bytes 23068672 | tf_op jit(solution)/shard_map/local_attention/pallas_call | solution.py:133
  57.7 1.3 copy-done
  59.1 0.6 copy-done.3
  59.7 35.1 %all-gather.6.cloned.1.call-done = bf16[128,64,512]{2,1,0:T(8,128)(2,1)} async-done(((bf16[4,64,512]{2,1,0:T(8,128)(2,1)}), bf16[128,64,512]{2,1,0:T(8,128)(2,1)}) %all-gather.6.cloned.1.call-update) | async-done | bytes 8388624 | tf_op jit(solution)/shard_map/all_gather | solution.py:209
  94.7 6.0 %fusion.12 = (bf16[32,2,64,512]{3,2,1,0:T(8,128)(2,1)}, bf16[32,2,64,512]{3,2,1,0:T(8,128)(2,1)}) fusion(bf16[32,4,64,512]{3,2,1,0:T(8,128)(2,1)} %bitcast.60), kind=kLoop, calls=%fused_computation.67 | loop fusion | bytes 16777216 | tf_op jit(solution)/shard_map/slice | solution.py:211
  100.7 12.3 %remote_attention.1 = (bf16[4,512,512]{2,1,0:T(8,128)(2,1)}, bf16[65,64,512]{2,1,0:T(8,128)(2,1)}, bf16[65,64,512]{2,1,0:T(8,128)(2,1)}) custom-call(s32[64]{0:T(128)} %broadcast_select_fusion.1.seq_ref, bf16[4,512,512]{2,1,0:T(8,128)(2,1)} %q_ref.3, bf16[4,512,512]{2,1,0:T(8,128)(2,1)} %do_ref.3, f32[4,4,512]{2,1,0:T(4,128)} %copy-done.2, ...), custom_call_target="tpu_custom_call" | custom-call | flops 10737418240 | bytes 29360128 | tf_op jit(solution)/shard_map/remote_attention/pallas_call | solution.py:158
  113.0 4.8 %slice.45 = bf16[64,64,512]{2,1,0:T(8,128)(2,1)} slice(bf16[65,64,512]{2,1,0:T(8,128)(2,1)} %get-tuple-element.15), slice={[0:64], [0:64], [0:512]} | slice | bytes 8388608 | tf_op jit(solution)/shard_map/slice | solution.py:233
  117.8 2.4 slice.46
  120.2 7.4 %pad_maximum_fusion = bf16[32,4,64,512]{3,2,1,0:T(8,128)(2,1)} fusion(bf16[32,2,64,512]{3,2,1,0:T(8,128)(2,1)} %bitcast.59, bf16[32,2,64,512]{3,2,1,0:T(8,128)(2,1)} %bitcast.58), kind=kLoop, calls=%fused_computation.2 | loop fusion | flops 4194304 | bytes 16777216 | tf_op jit(solution)/shard_map/concatenate | solution.py:232
  127.7 0.5 all-gather.4.cloned.1.call-update
  128.3 0.2 reduce-scatter.7.cloned.1.call-start
  129.1 112.2 %reduce-scatter.5.cloned.1.call-done = bf16[1,4,64,512]{3,2,1,0:T(8,128)(2,1)} async-done(((bf16[32,4,64,512]{3,2,1,0:T(8,128)(2,1)}), bf16[1,4,64,512]{3,2,1,0:T(8,128)(2,1)}) %reduce-scatter.5.cloned.1.call-update) | async-done | bytes 262160 | tf_op jit(solution)/shard_map/reduce_scatter | solution.py:234
  241.2 1.0 convert_element_type.37
  242.3 0.5 mul.124
  242.8 0.5 mul.116
  243.4 0.5 mul.132
  243.9 0.5 mul.128
  244.4 0.5 copy-done.1
  244.9 3.1 fusion.1
  248.1 10.5 %convolution_bitcast_fusion = f32[2048,512]{0,1:T(8,128)} fusion(bf16[4,512,512]{2,1,0:T(8,128)(2,1)} %get-tuple-element.50, bf16[4,512,2048]{2,1,0:T(8,128)(2,1)} %all-gather.4.cloned.1.call-done), kind=kOutput, calls=%fused_computation.13 | convolution fusion | flops 4294967296 | bytes 14680064 | tf_op jit(solution)/shard_map/dot_general | solution.py:246
  258.6 5.3 %copy.49 = f32[2048,512]{1,0:T(8,128)} copy(f32[2048,512]{0,1:T(8,128)} %convolution_bitcast_fusion) | data formatting | bytes 8388608
  263.9 81.8 %reduce-scatter.7.cloned.1.call-done = f32[64,512]{1,0:T(8,128)} async-done(((f32[2048,512]{1,0:T(8,128)}), f32[64,512]{1,0:T(8,128)}) %reduce-scatter.7.cloned.1.call-update) | async-done | bytes 131088
  (59 shorter events, 2.9 us)
Async XLA Ops:
  8.0 36.0 %copy-start.5 = (s32[4,8,12]{2,1,0:T(8,128)S(1)}, s32[4,8,12]{2,1,0:T(8,128)}, u32[]{:S(2)}) copy-start(s32[4,8,12]{2,1,0:T(8,128)} %param.15) | copy-start | bytes 4612
  8.0 37.5 %copy-start.6 = (f32[4,512,4]{1,2,0:T(4,128)S(1)}, f32[4,512,4]{1,2,0:T(4,128)}, u32[]{:S(2)}) copy-start(f32[4,512,4]{1,2,0:T(4,128)} %param.14) | copy-start | bytes 98308
  8.0 86.7 %all-gather.6.cloned.1.call-start = ((), (), s32[]{:S(2)}) async-start(), calls=%async_computation.4 | async-start | bytes 8650752 | tf_op jit(solution)/shard_map/all_gather | solution.py:209
  42.5 198.8 %reduce-scatter.5.cloned.1.call-start = ((), (), s32[]{:S(2)}) async-start(), calls=%async_computation.2 | async-start | bytes 8650752 | tf_op jit(solution)/shard_map/reduce_scatter | solution.py:234
  45.5 12.2 %copy-start.2 = (f32[4,4,512]{2,1,0:T(4,128)}, f32[4,4,512]{2,1,0:T(4,128)S(1)}, u32[]{:S(2)}) copy-start(f32[4,4,512]{2,1,0:T(4,128)S(1)} %multiply_bitcast_fusion.lse_ref) | copy-start | bytes 98308
  57.7 1.3 copy-start
  59.1 0.6 copy-start.3
  113.0 4.8 %copy-start.4 = (bf16[65,64,512]{2,1,0:T(8,128)(2,1)S(1)}, bf16[65,64,512]{2,1,0:T(8,128)(2,1)}, u32[]{:S(2)}) copy-start(bf16[65,64,512]{2,1,0:T(8,128)(2,1)} %get-tuple-element.16) | copy-start | bytes 12779524
  127.7 120.4 %all-gather.4.cloned.1.call-start = ((), (), s32[]{:S(2)}) async-start(), calls=%async_computation.3 | async-start | bytes 10485760 | tf_op jit(solution)/shard_map/all_gather | solution.py:245
  128.3 217.5 %reduce-scatter.7.cloned.1.call-start = ((), (), s32[]{:S(2)}) async-start(), calls=%async_computation.5 | async-start | bytes 4325376
  243.3 1.6 copy-start.1
Sparse Core Ops, SparseCore 0:
  42.6 52.0 all-gather.5
  127.8 113.3 reduce-scatter.4
  264.0 81.6 reduce-scatter.6
Sparse Core Ops, SparseCore 1:
  129.8 103.2 all-gather.3

commit v2 on v1

v2 whole, which is shorter than its diff:
```python
import functools
import jax
import jax.numpy as jnp
from jax import lax
from jax.experimental import pallas as pl
from jax.experimental.pallas import tpu as pltpu
from jax.sharding import PartitionSpec as P

BLK = 64
CAP = 2
DH = 128
LOG2E = 1.4426950408889634
ROOT = DH ** -0.5
BIG = 1e30

NT = (((1,), (1,)), ((), ()))
TN = (((0,), (0,)), ((), ()))
NN = (((1,), (0,)), ((), ()))


def mm(a, b, dims):
    return lax.dot_general(a, b, dims, preferred_element_type=jnp.float32)


class Net:
    def __init__(self, send, recv):
        self.send, self.recv, self.n, self.all = send, recv, 0, []

    def copy(self, src, dst, kv):
        i = self.n
        self.n += 1
        c = pltpu.make_async_remote_copy(
            src_ref=src, dst_ref=dst, send_sem=self.send.at[i], recv_sem=self.recv.at[i],
            device_id=(kv, lax.axis_index("tp")), device_id_type=pl.DeviceIdType.MESH)
        c.start()
        self.all.append(c)
        return c

    def finish(self):
        for c in self.all:
            c.wait_send()


class Disk:
    def __init__(self, sems):
        self.sems, self.n, self.all = sems, 0, []

    def copy(self, src, dst):
        c = pltpu.make_async_copy(src, dst, self.sems.at[self.n])
        self.n += 1
        c.start()
        return c

    def keep(self, src, dst):
        self.all.append(self.copy(src, dst))

    def finish(self):
        for c in self.all:
            c.wait()


def place():
    me = lax.axis_index("kv")
    return me // 8, (me // 2) % 4, me % 2


def kv_of(z, y, c):
    return (z * 4 + y) * 2 + c


def barrier_with(peers):
    sem = pltpu.get_barrier_semaphore()
    for kv in peers:
        pl.semaphore_signal(sem, inc=1, device_id=(kv, lax.axis_index("tp")),
                            device_id_type=pl.DeviceIdType.MESH)
    pl.semaphore_wait(sem, len(peers))


class Gather:
    def __init__(self, net, disk, buf, out, cut, y_first):
        z, y, c = place()
        self.net, self.disk, self.buf, self.out, self.cut, self.y_first = net, disk, buf, out, cut, y_first
        f, s = (y, z) if y_first else (z, y)
        self.c = c
        self.f = [f, (f + 3) % 4, (f + 1) % 4, (f + 2) % 4]
        self.s = [s, (s + 3) % 4, (s + 1) % 4, (s + 2) % 4]
        self.side = []

    def at(self, f, s, c):
        return (c, s, f) if self.y_first else (c, f, s)

    def dev(self, f, s, c):
        return kv_of(s, f, c) if self.y_first else kv_of(f, s, c)

    def full(self, f, s, c=None):
        return self.buf.at[self.at(f, s, self.c if c is None else c)]

    def half(self, f, s, which):
        rows = pl.ds(0, self.cut) if which == 0 else pl.ds(self.cut, self.buf.shape[3] - self.cut)
        return self.buf.at[self.at(f, s, self.c) + (rows,)]

    def send(self, ref, f, s):
        return self.net.copy(ref, ref, self.dev(f, s, self.c))

    def have(self, f, s):
        ref = self.full(f, s)
        self.side.append((f, s, self.net.copy(ref, ref, self.dev(self.f[0], self.s[0], 1 - self.c))))
        self.disk.keep(ref, self.out.at[self.at(f, s, self.c)])

    def across(self, f):
        return (self.send(self.full(f, self.s[0]), self.f[0], self.s[2]),
                self.send(self.full(f, self.s[0]), self.f[0], self.s[1]))

    def phase0(self):
        own = self.full(self.f[0], self.s[0])
        self.a = self.send(own, self.f[2], self.s[0])
        self.b = self.send(own, self.f[1], self.s[0])
        self.second = [self.across(self.f[0])]
        self.have(self.f[0], self.s[0])

    def phase1(self):
        self.a.wait_recv()
        self.e = self.send(self.half(self.f[1], self.s[0], 0), self.f[2], self.s[0])
        self.second.append(self.across(self.f[1]))
        self.b.wait_recv()
        self.g = self.send(self.half(self.f[2], self.s[0], 1), self.f[1], self.s[0])
        self.second.append(self.across(self.f[2]))
        self.have(self.f[1], self.s[0])
        self.have(self.f[2], self.s[0])

    def phase2(self):
        self.e.wait_recv()
        self.g.wait_recv()
        self.second.append(self.across(self.f[3]))
        self.have(self.f[3], self.s[0])
        self.last = []

    def phase3(self, j):
        up, down = self.second[j]
        up.wait_recv()
        p = self.send(self.half(self.f[j], self.s[1], 0), self.f[0], self.s[2])
        down.wait_recv()
        q = self.send(self.half(self.f[j], self.s[2], 1), self.f[0], self.s[1])
        self.last.append((p, q))
        self.have(self.f[j], self.s[1])
        self.have(self.f[j], self.s[2])

    def phase4(self, j):
        for c in self.last[j]:
            c.wait_recv()
        self.have(self.f[j], self.s[3])

    def phase5(self):
        for f, s, c in self.side:
            c.wait_recv()
            self.disk.keep(self.full(f, s, 1 - self.c), self.out.at[self.at(f, s, 1 - self.c)])


def gather_kernel(need, lse_ref, sel_ref, q_hbm, k_hbm, v_hbm, o_hbm, do_hbm,
                  dqt_hbm, dk_hbm, dv_hbm, delta_ref, pk_hbm, pv_hbm, hot_ref,
                  qb, kb, vb, ob, dob, dqtb, dkb, dvb, pk, pv, rc, n1, ry, n2, rz,
                  send, recv, local):
    z, y, c = place()
    net, disk = Net(send, recv), Disk(local)
    loads = [disk.copy(a, b) for a, b in
             ((k_hbm, kb), (v_hbm, vb), (q_hbm, qb), (do_hbm, dob), (o_hbm, ob))]
    peers = [kv_of(z, y, 1 - c)]
    for d in range(1, 4):
        peers += [kv_of(z, (y + d) % 4, c), kv_of((z + d) % 4, y, c)]
    barrier_with(peers)
    first = net.copy(need.at[1 - c], rc, kv_of(z, y, 1 - c))
    for l in loads:
        l.wait()

    seqs, n, ch = qb.shape
    half = n // 2

    def unit(u, _):
        s = u // 2
        for g in range(2):
            h = (u % 2) * 2 + g
            hs = pl.ds(pl.multiple_of(h * DH, DH), DH)
            hr = pl.ds(h, 1)
            q = qb[s, :, hs]
            do = dob[s, :, hs]
            prod = do.astype(jnp.float32) * ob[s, :, hs].astype(jnp.float32)
            delta = jnp.sum(prod.T, axis=0, keepdims=True)
            delta_ref[s, hr, :] = delta
            lse = lse_ref[s, hr, :]
            parts = []
            for t in range(2):
                lo = t * half
                k = kb[s, pl.ds(lo, half), hs]
                v = vb[s, pl.ds(lo, half), hs]
                qc, doc = q[lo:], do[lo:]
                w = n - lo
                sc = mm(k, qc, NT)
                row = lax.broadcasted_iota(jnp.int32, (half, w), 0)
                col = lax.broadcasted_iota(jnp.int32, (half, w), 1)
                bias = jnp.concatenate(
                    [jnp.broadcast_to(lse[:, lo:] + sel_ref[s, j:j + 1, lo:], (BLK, w))
                     for j in range(lo // BLK, (lo + half) // BLK)], axis=0)
                p = jnp.exp2(jnp.where(row <= col, sc * (ROOT * LOG2E) - bias, -BIG))
                dp = mm(v, doc, NT)
                ds = (p * (dp - delta[:, lo:])).astype(jnp.bfloat16)
                dvb[s, pl.ds(lo, half), hs] = mm(p.astype(jnp.bfloat16), doc, NN).astype(jnp.bfloat16)
                dkb[s, pl.ds(lo, half), hs] = (mm(ds, qc, NN) * ROOT).astype(jnp.bfloat16)
                parts.append(mm(k, ds, TN))
            dqtb[s, hs, :half] = parts[0][:, :half]
            dqtb[s, hs, half:] = parts[0][:, half:] + parts[1]
        return 0

    def units(a, b):
        lax.fori_loop(a, b, unit, 0)

    units(0, 1)
    first.wait_recv()
    n1[...] = jnp.maximum(need[c], rc[...])
    ys = [net.copy(n1.at[(y + d) % 4], ry.at[d - 1], kv_of(z, (y + d) % 4, c)) for d in range(1, 4)]
    units(1, 2)
    for x in ys:
        x.wait_recv()
    n2[...] = jnp.maximum(jnp.maximum(n1[y], ry[0]), jnp.maximum(ry[1], ry[2]))
    zs = [net.copy(n2.at[(z + d) % 4], rz.at[d - 1], kv_of((z + d) % 4, y, c)) for d in range(1, 4)]
    units(2, 3)
    for x in zs:
        x.wait_recv()
    need1 = jnp.maximum(jnp.maximum(n2[z], rz[0]), jnp.maximum(rz[1], rz[2]))
    tri = (lax.broadcasted_iota(jnp.int32, (128, 128), 0) <=
           lax.broadcasted_iota(jnp.int32, (128, 128), 1))
    count = mm(need1.astype(jnp.bfloat16), tri.astype(jnp.float32).astype(jnp.bfloat16), NN)
    is0 = jnp.where((need1 > 0.5) & (count > 0.5) & (count < 1.5), 1.0, 0.0)
    is1 = jnp.where((need1 > 0.5) & (count > 1.5) & (count < 2.5), 1.0, 0.0)
    line = lax.broadcasted_iota(jnp.int32, (16, 128), 0)
    hot = jnp.where(line == 0, jnp.broadcast_to(is0[0:1], (16, 128)),
                    jnp.where(line == 1, jnp.broadcast_to(is1[0:1], (16, 128)), 0.0))
    hot = hot.astype(jnp.bfloat16)
    hot_ref[...] = hot
    pick_k = jnp.zeros((2 * BLK, ch), jnp.float32)
    pick_v = jnp.zeros((2 * BLK, ch), jnp.float32)
    for s in range(seqs):
        a = spread(hot, s, n)
        pick_k = pick_k + mm(a, kb[s], NN)
        pick_v = pick_v + mm(a, vb[s], NN)
    pk[c, z, y, :BLK] = pick_k[:BLK].astype(jnp.bfloat16)
    pk[c, z, y, BLK + 16:] = pick_k[BLK:].astype(jnp.bfloat16)
    pk[c, z, y, BLK:BLK + 16] = jnp.concatenate([hot] * (ch // 128), axis=1)
    pv[c, z, y] = pick_v.astype(jnp.bfloat16)

    gs = [Gather(net, disk, pk, pk_hbm, BLK + 16, True), Gather(net, disk, pv, pv_hbm, BLK, False)]
    for g in gs:
        g.phase0()
    units(3, 5)
    for g in gs:
        g.phase1()
    units(5, 6)
    for g in gs:
        g.phase2()
    for j in range(4):
        if j < 2:
            units(6 + j, 7 + j)
        for g in gs:
            g.phase3(j)
        if j == 1:
            disk.keep(dqtb, dqt_hbm)
            disk.keep(dkb, dk_hbm)
            disk.keep(dvb, dv_hbm)
    for j in range(4):
        for g in gs:
            g.phase4(j)
    for g in gs:
        g.phase5()
    net.finish()
    disk.finish()


def spread(hot, s, n):
    blocks = n // BLK
    b = lax.broadcasted_iota(jnp.int32, (128, n), 0)
    l = lax.broadcasted_iota(jnp.int32, (128, n), 1)
    rep = jnp.where(b == s * blocks + l // BLK, 1.0, 0.0).astype(jnp.bfloat16)
    wide = mm(hot, rep, NN)
    wide = jnp.where(b < BLK, jnp.broadcast_to(wide[0:1], (128, n)), jnp.broadcast_to(wide[1:2], (128, n)))
    return jnp.where(b % BLK == l % BLK, wide, 0.0).astype(jnp.bfloat16)


def gather_attention(need, lse, sel, q, k, v, o, do):
    seqs, n, ch = q.shape
    heads = ch // DH
    bf, f32 = jnp.bfloat16, jnp.float32
    whole = pl.BlockSpec(memory_space=pltpu.VMEM)
    hbm = pl.BlockSpec(memory_space=pl.ANY)
    return pl.pallas_call(
        gather_kernel,
        in_specs=[whole] * 3 + [hbm] * 5,
        out_specs=[hbm, hbm, hbm, whole, hbm, hbm, whole],
        out_shape=[
            jax.ShapeDtypeStruct((seqs, ch, n), f32),
            jax.ShapeDtypeStruct(q.shape, bf),
            jax.ShapeDtypeStruct(q.shape, bf),
            jax.ShapeDtypeStruct((seqs, heads, n), f32),
            jax.ShapeDtypeStruct((2, 4, 4, 2 * BLK + 16, ch), bf),
            jax.ShapeDtypeStruct((2, 4, 4, 2 * BLK, ch), bf),
            jax.ShapeDtypeStruct((16, 128), bf),
        ],
        scratch_shapes=[pltpu.VMEM(q.shape, bf)] * 5 + [
            pltpu.VMEM((seqs, ch, n), f32), pltpu.VMEM(q.shape, bf), pltpu.VMEM(q.shape, bf),
            pltpu.VMEM((2, 4, 4, 2 * BLK + 16, ch), bf), pltpu.VMEM((2, 4, 4, 2 * BLK, ch), bf),
            pltpu.VMEM((4, 4, 8, 128), f32), pltpu.VMEM((4, 4, 8, 128), f32),
            pltpu.VMEM((3, 4, 8, 128), f32), pltpu.VMEM((4, 8, 128), f32), pltpu.VMEM((3, 8, 128), f32),
            pltpu.SemaphoreType.DMA((80,)), pltpu.SemaphoreType.DMA((80,)), pltpu.SemaphoreType.DMA((80,)),
        ],
        compiler_params=pltpu.CompilerParams(
            vmem_limit_bytes=56 * 1024 * 1024, collective_id=0, has_side_effects=True),
        cost_estimate=pl.CostEstimate(flops=20_000_000_000, bytes_accessed=30 << 20, transcendentals=1 << 22),
        name="gather_attention",
    )(need, lse, sel, q, k, v, o, do)


class Route:
    def __init__(self, net, buf, rows, y_first, slots):
        z, y, c = place()
        self.net, self.buf, self.rows, self.y_first = net, buf, rows, y_first
        self.ra, self.rb, self.rp, self.rm, self.e, self.ta, self.tb, self.tp, self.tm = slots
        f, s = (y, z) if y_first else (z, y)
        self.c, self.f, self.s = c, f, s
        self.wide = buf.shape[-1] // 2

    def dev(self, f, s):
        return kv_of(s, f, self.c) if self.y_first else kv_of(f, s, self.c)

    def src(self, f, part=None):
        lanes = pl.ds(0, 2 * self.wide) if part is None else pl.ds(part * self.wide, self.wide)
        if self.y_first:
            return self.buf.at[:, f, self.rows, lanes]
        return self.buf.at[f, :, self.rows, lanes]

    def step1(self):
        f, s = self.f, self.s
        self.c1 = (self.net.copy(self.src((f + 2) % 4, 0), self.ra, self.dev((f + 1) % 4, s)),
                   self.net.copy(self.src((f + 2) % 4, 1), self.rb, self.dev((f + 3) % 4, s)))

    def step2(self):
        f, s, w = self.f, self.s, self.wide
        self.c2 = []
        for i, (d, got, dst) in enumerate(((1, self.ra, self.rp), (3, self.rb, self.rm))):
            self.c1[i].wait_recv()
            at = self.src((f + d) % 4, i)
            at[...] = (at[...].astype(jnp.float32) + got[...].astype(jnp.float32)).astype(jnp.bfloat16)
            self.c2.append(self.net.copy(self.src((f + d) % 4), dst, self.dev((f + d) % 4, s)))

    def step3(self):
        f, s, w = self.f, self.s, self.wide
        for x in self.c2:
            x.wait_recv()
        total = self.src(f)[...].astype(jnp.float32) + self.rp[...].astype(jnp.float32)
        self.e[...] = (total + self.rm[...].astype(jnp.float32)).astype(jnp.bfloat16)
        far = (s + 2) % 4
        self.c3 = (self.net.copy(self.e.at[far, :, pl.ds(0, w)], self.ta, self.dev(f, (s + 1) % 4)),
                   self.net.copy(self.e.at[far, :, pl.ds(w, w)], self.tb, self.dev(f, (s + 3) % 4)))

    def step4(self):
        f, s, w = self.f, self.s, self.wide
        self.c4 = []
        for i, (d, got, dst) in enumerate(((1, self.ta, self.tp), (3, self.tb, self.tm))):
            self.c3[i].wait_recv()
            at = self.e.at[(s + d) % 4, :, pl.ds(i * w, w)]
            at[...] = (at[...].astype(jnp.float32) + got[...].astype(jnp.float32)).astype(jnp.bfloat16)
            self.c4.append(self.net.copy(self.e.at[(s + d) % 4], dst, self.dev(f, (s + d) % 4)))

    def step5(self):
        for x in self.c4:
            x.wait_recv()
        total = self.e[self.s].astype(jnp.float32) + self.tp[...].astype(jnp.float32)
        return total + self.tm[...].astype(jnp.float32)


def route_scratch(rows, ch):
    bf = jnp.bfloat16
    return [pltpu.VMEM((4, rows, ch // 2), bf), pltpu.VMEM((4, rows, ch // 2), bf),
            pltpu.VMEM((4, rows, ch), bf), pltpu.VMEM((4, rows, ch), bf), pltpu.VMEM((4, rows, ch), bf),
            pltpu.VMEM((rows, ch // 2), bf), pltpu.VMEM((rows, ch // 2), bf),
            pltpu.VMEM((rows, ch), bf), pltpu.VMEM((rows, ch), bf)]


class Stream:
    def __init__(self, net, buf, slots):
        rows = buf.shape[2] // 2
        self.rows = rows
        self.routes = [Route(net, buf, pl.ds(0, rows), True, slots[:9]),
                       Route(net, buf, pl.ds(rows, rows), False, slots[9:])]

    def run(self, name):
        return [getattr(r, name)() for r in self.routes]


def reduce_kernel(hot_ref, gk_hbm, gv_hbm, dv_hbm, x_hbm, fk_ref, fv_ref, dw_ref,
                  mk, mv, rk, rv, dvb, xb, wf, ws, wr, wb, *rest):
    ks, vs, wslots = rest[0:18], rest[18:36], rest[36:54]
    send, recv, local = rest[54:]
    z, y, c = place()
    net, disk = Net(send, recv), Disk(local)
    mine, other = pl.ds(c * 16, 16), pl.ds((1 - c) * 16, 16)
    load_v = disk.copy(gv_hbm.at[mine], mv)
    load_k = disk.copy(gk_hbm.at[mine], mk)
    load_d = disk.copy(dv_hbm, dvb)
    load_x = [disk.copy(x_hbm.at[t], xb.at[t]) for t in range(4)]
    peers = [kv_of(z, y, 1 - c)]
    for d in (1, 3):
        peers += [kv_of(z, (y + d) % 4, c), kv_of((z + d) % 4, y, c)]
    barrier_with(peers)
    partner = kv_of(z, y, 1 - c)
    side_v = net.copy(gv_hbm.at[other], rv, partner)
    side_k = net.copy(gk_hbm.at[other], rk, partner)

    def fold(dst, src, parts):
        def step(i, _):
            dst[i] = (dst[i].astype(jnp.float32) + src[i].astype(jnp.float32)).astype(jnp.bfloat16)
            return 0
        lax.fori_loop(0, parts, step, 0)

    bv = mv.reshape(4, 4, mv.shape[1], mv.shape[2])
    bk = mk.reshape(4, 4, mk.shape[1], mk.shape[2])
    v, k = Stream(net, bv, vs), Stream(net, bk, ks)
    seqs, n, ch = dvb.shape

    def product(t):
        load_x[t].wait()

        def step(s, _):
            wf[t] = wf[t] + mm(xb[t, s], dvb[s], TN)
            return 0

        wf[t] = mm(xb[t, 0], dvb[0], TN)
        lax.fori_loop(1, seqs, step, 0)

    load_v.wait()
    side_v.wait_recv()
    fold(mv, rv, 16)
    v.run("step1")
    load_k.wait()
    side_k.wait_recv()
    fold(mk, rk, 16)
    k.run("step1")
    load_d.wait()
    hot = hot_ref[...]
    v.run("step2")
    product(0)
    k.run("step2")
    product(1)
    v.run("step3")
    product(2)
    v.run("step4")
    product(3)
    old = jnp.zeros((2 * BLK, ch), jnp.float32)
    xs = [jnp.zeros((2 * BLK, ch), jnp.float32) for t in range(4)]
    for s in range(seqs):
        a = spread(hot, s, n)
        old = old + mm(a, dvb[s], NN)
        xs = [x + mm(a, xb[t, s], NN) for t, x in enumerate(xs)]
    top, low = v.run("step5")
    fv_ref[:BLK] = top
    fv_ref[BLK:] = low
    extra = jnp.concatenate([top, low], axis=0)
    diff = ((old + extra).astype(jnp.bfloat16).astype(jnp.float32) - old).astype(jnp.bfloat16)
    for t in range(4):
        wf[t] = wf[t] + mm(xs[t].astype(jnp.bfloat16), diff, TN)
        for j in range(4):
            ws[t * 4 + j] = wf[t, pl.ds(pl.multiple_of(j * 128 + (1 - c) * BLK, BLK), BLK)].astype(jnp.bfloat16)
    side_w = net.copy(ws, wr, partner)
    k.run("step3")
    side_w.wait_recv()
    for t in range(4):
        for j in range(4):
            own = wf[t, pl.ds(pl.multiple_of(j * 128 + c * BLK, BLK), BLK)]
            wb[t, j] = (own + wr[t * 4 + j].astype(jnp.float32)).astype(jnp.bfloat16)
    w = Stream(net, wb, wslots)
    w.run("step1")
    k.run("step4")
    w.run("step2")
    top, low = k.run("step5")
    fk_ref[:BLK] = top
    fk_ref[BLK:] = low
    w.run("step3")
    w.run("step4")
    top, low = w.run("step5")
    dw_ref[:BLK // 2] = top
    dw_ref[BLK // 2:] = low
    net.finish()


def reduce_weight(hot, gk, gv, dv, x):
    seqs, n, ch = dv.shape
    bf, f32 = jnp.bfloat16, jnp.float32
    whole = pl.BlockSpec(memory_space=pltpu.VMEM)
    hbm = pl.BlockSpec(memory_space=pl.ANY)
    part = pltpu.VMEM((16, 2 * BLK, ch), bf)
    return pl.pallas_call(
        reduce_kernel,
        in_specs=[whole] + [hbm] * 4,
        out_specs=[whole] * 3,
        out_shape=[
            jax.ShapeDtypeStruct((2 * BLK, ch), f32),
            jax.ShapeDtypeStruct((2 * BLK, ch), f32),
            jax.ShapeDtypeStruct((BLK, ch), f32),
        ],
        scratch_shapes=[part] * 4 + [
            pltpu.VMEM(dv.shape, bf), pltpu.VMEM(x.shape, bf), pltpu.VMEM((4, n, ch), f32),
            pltpu.VMEM((16, BLK, ch), bf), pltpu.VMEM((16, BLK, ch), bf), pltpu.VMEM((4, 4, BLK, ch), bf),
        ] + route_scratch(BLK, ch) * 4 + route_scratch(BLK // 2, ch) * 2 + [
            pltpu.SemaphoreType.DMA((60,)), pltpu.SemaphoreType.DMA((60,)), pltpu.SemaphoreType.DMA((8,)),
        ],
        compiler_params=pltpu.CompilerParams(
            vmem_limit_bytes=56 * 1024 * 1024, collective_id=1, has_side_effects=True),
        cost_estimate=pl.CostEstimate(flops=20_000_000_000, bytes_accessed=20 << 20, transcendentals=0),
        name="reduce_weight",
    )(hot, gk, gv, dv, x)


def remote_kernel(seq_ref, q_ref, do_ref, lse_ref, delta_ref, sel_ref, pk_ref, pv_ref, dqt_in,
                  dq_ref, gk_ref, gv_ref, acc, list_ref, cnt_ref):
    seqs = 4
    heads = q_ref.shape[2] // DH
    slots = 2 * pk_ref.shape[0]
    s = pl.program_id(0)

    @pl.when(s == 0)
    def _():
        for t in range(seqs):
            cnt_ref[t] = 0

        def scan(i, _):
            t = seq_ref[i]

            @pl.when(t >= 0)
            def _():
                c = cnt_ref[t]
                list_ref[t, c] = i
                cnt_ref[t] = c + 1

            @pl.when(t < 0)
            def _():
                gk_ref[i] = jnp.zeros(gk_ref.shape[1:], gk_ref.dtype)
                gv_ref[i] = jnp.zeros(gv_ref.shape[1:], gv_ref.dtype)
            return 0

        lax.fori_loop(0, slots, scan, 0)

    acc[...] = dqt_in[0]
    n = cnt_ref[s]

    def chunk(c, _):
        ids = []
        for e in range(4):
            at = c * 4 + e
            i = list_ref[s, jnp.minimum(at, n - 1)]
            ids.append((i, jnp.where(at < n, i, slots)))
        for h in range(heads):
            hs = slice(h * DH, (h + 1) * DH)
            q = q_ref[0, :, hs]
            do = do_ref[0, :, hs]
            k = jnp.concatenate([pk_ref[i // 2, pl.ds(pl.multiple_of(i % 2 * 80, 16), BLK), hs] for i, _ in ids], axis=0)
            v = jnp.concatenate([pv_ref[i // 2, pl.ds(pl.multiple_of(i % 2 * BLK, BLK), BLK), hs] for i, _ in ids], axis=0)
            lse = lse_ref[0, h:h + 1, :]
            st = mm(k, q, NT)
            bias = jnp.concatenate(
                [jnp.broadcast_to(lse + sel_ref[j], (BLK, lse.shape[1])) for _, j in ids], axis=0)
            p = jnp.exp2(st * (ROOT * LOG2E) - bias)
            dp = mm(v, do, NT)
            ds = (p * (dp - delta_ref[0, h:h + 1, :])).astype(jnp.bfloat16)
            dv = mm(p.astype(jnp.bfloat16), do, NN).astype(jnp.bfloat16)
            dk = (mm(ds, q, NN) * ROOT).astype(jnp.bfloat16)
            for e, (_, j) in enumerate(ids):
                gv_ref[j, :, hs] = dv[e * BLK:(e + 1) * BLK]
                gk_ref[j, :, hs] = dk[e * BLK:(e + 1) * BLK]
            acc[hs, :] += mm(k, ds, TN)
        return 0

    lax.fori_loop(0, (n + 3) // 4, chunk, 0)
    for h in range(heads):
        hs = slice(h * DH, (h + 1) * DH)
        dq_ref[0, :, hs] = (acc[hs, :].T * ROOT).astype(jnp.bfloat16)


def remote_attention(slot_seq, q, do, lse, delta, sel, pk, pv, dqt):
    seqs, n, ch = q.shape
    heads = ch // DH
    slots = 2 * pk.shape[0]
    big = pl.BlockSpec((1, n, ch), lambda s: (s, 0, 0))
    small = pl.BlockSpec((1, heads, n), lambda s: (s, 0, 0))
    whole = pl.BlockSpec(memory_space=pltpu.VMEM)
    return pl.pallas_call(
        remote_kernel,
        grid=(seqs,),
        in_specs=[pl.BlockSpec(memory_space=pltpu.SMEM), big, big, small, small, whole, whole, whole,
                  pl.BlockSpec((1, ch, n), lambda s: (s, 0, 0))],
        out_specs=[big, whole, whole],
        out_shape=[
            jax.ShapeDtypeStruct(q.shape, jnp.bfloat16),
            jax.ShapeDtypeStruct((slots + 2, BLK, ch), jnp.bfloat16),
            jax.ShapeDtypeStruct((slots + 2, BLK, ch), jnp.bfloat16),
        ],
        scratch_shapes=[
            pltpu.VMEM((ch, n), jnp.float32),
            pltpu.SMEM((seqs, slots), jnp.int32),
            pltpu.SMEM((seqs,), jnp.int32),
        ],
        compiler_params=pltpu.CompilerParams(vmem_limit_bytes=60 * 1024 * 1024),
        cost_estimate=pl.CostEstimate(flops=5 * 2 * heads * slots * BLK * n * DH, bytes_accessed=28 << 20,
                                      transcendentals=heads * slots * BLK * n),
        name="remote_attention",
    )(slot_seq, q, do, lse, delta, sel, pk, pv, dqt)


def body(layer_input, queries, keys, values, outputs, d_out, log_sums, chosen):
    seqs, n, ch = queries.shape
    local_blocks = n // BLK
    devices = lax.axis_size("kv")
    me = lax.axis_index("kv")
    own = seqs * local_blocks
    lse = jnp.swapaxes(log_sums, 1, 2) * LOG2E
    whole = lax.all_gather(layer_input, "tp", axis=0)

    in_use = chosen >= 0
    remote = in_use & (chosen // local_blocks != me)
    ids = jnp.arange(devices * local_blocks, dtype=jnp.int32)
    needed = jnp.max(((chosen[..., None] == ids) & remote[..., None]).astype(jnp.float32), axis=(1, 2))
    needed = needed.reshape(seqs, 4, 4, 2, local_blocks).transpose(3, 2, 1, 0, 4).reshape(2, 4, 4, 1, own)
    needed = jnp.pad(jnp.broadcast_to(needed, (2, 4, 4, 8, own)), ((0, 0),) * 4 + ((0, 128 - own),))
    mine = me * local_blocks + jnp.arange(local_blocks, dtype=jnp.int32)
    picked = jnp.any(chosen[:, None, :, :] == mine[None, :, None, None], axis=3)
    sel_local = jnp.repeat(jnp.where(picked, 0.0, BIG).astype(jnp.float32), BLK, axis=2)
    dqt, dk_local, dv_local, delta, pk, pv, hot = gather_attention(
        needed, lse, sel_local, queries, keys, values, outputs, d_out)

    pk = pk.reshape(devices, 2 * BLK + 16, ch)
    pv = pv.reshape(devices, 2 * BLK, ch)
    table = pk[:, BLK:BLK + CAP, :own].astype(jnp.float32)
    place_of = jnp.sum(table * jnp.arange(own, dtype=jnp.float32), axis=2).astype(jnp.int32)
    flat = jnp.where(jnp.sum(table, axis=2) > 0.5, place_of, -1).reshape(devices * CAP)
    order = jnp.arange(devices * CAP, dtype=jnp.int32) // CAP
    owner = (order % (devices // 2)) * 2 + order // (devices // 2)
    slot_seq = jnp.where(flat >= 0, flat // local_blocks, -1)
    slot_id = jnp.where(flat >= 0, owner * local_blocks + flat % local_blocks, -2)
    named = jnp.any(chosen[:, None] == slot_id[None, :, None, None], axis=3)
    named = named & (slot_seq[None, :, None] == jnp.arange(seqs, dtype=jnp.int32)[:, None, None])
    named = jnp.any(named, axis=0) & (owner != me)[:, None]
    slot_seq = jnp.where(jnp.any(named, axis=1), slot_seq, -1)
    sel_remote = jnp.repeat(jnp.where(named, 0.0, BIG).astype(jnp.float32), BLK, axis=1)
    sel_remote = jnp.concatenate([sel_remote, jnp.full((8, n), BIG, jnp.float32)], axis=0)[:, None, :]
    d_queries, gk, gv = remote_attention(slot_seq, queries, d_out, lse, delta, sel_remote, pk, pv, dqt)

    gk = gk.reshape(devices + 1, CAP * BLK, ch)
    gv = gv.reshape(devices + 1, CAP * BLK, ch)
    back_k, back_v, d_weight = reduce_weight(hot, gk, gv, dv_local, whole)
    serve = hot[:CAP, :own].astype(jnp.float32)

    def finish(local, extra):
        full = local.reshape(own, BLK, ch).astype(jnp.float32)
        for c in range(CAP):
            full = full + serve[c][:, None, None] * extra[c * BLK:(c + 1) * BLK][None]
        return full.astype(jnp.bfloat16).reshape(seqs, n, ch)

    return d_queries, finish(dk_local, back_k), finish(dv_local, back_v), d_weight


def solution(mesh):
    spec = P(None, "kv", "tp")
    return jax.shard_map(
        body,
        mesh=mesh,
        in_specs=(spec,) * 7 + (P(None, "kv", None),),
        out_specs=(spec, spec, spec, P("kv", "tp")),
        check_vma=False,
    )
```

time: 353 us -> 169 us (0.48)
  waiting for transfers between devices: 230 us -> 15.9 us
  Pallas kernels: 24.5 us -> 119 us
  blocking collectives: 26.4 us -> 0 us
  local copies, waits for them, and re-layouts: 30.7 us -> 9.46 us
  matrix products: 10.5 us -> 0 us
  other arithmetic: 15.3 us -> 9.13 us
    reduce_scatter x1 -> x0, waiting for transfers between devices: 112 us -> none  [body(): back = lax.psum_scatter(back, 'kv', scatter_dimension=0).astype(jnp.float32)]
    pallas_call x1 -> x2, Pallas kernels: 12.2 us -> 107 us  [the longest x1 57.9 us: reduce_weight(): pl.pallas_call(reduce_kernel, in_specs=[whole] + [hbm] * 4, out_specs=[wh...]
    unnamed x5 -> x1, waiting for transfers between devices: 82.4 us -> 0.68 us
    all_gather x1 -> x0, blocking collectives: 26.4 us -> none  [body(): everyone = lax.all_gather(needed, 'kv').max(axis=0)]
    all_gather x2 -> x1, waiting for transfers between devices: 35.1 us -> 15.3 us  [body(): whole = lax.all_gather(layer_input, 'tp', axis=0)]
    slice x4 -> x2, local copies, waits for them, and re-layouts: 13.2 us -> 1.15 us  [finish(): full = full + serve[c][:, None, None] * extra[c * BLK:(c + 1) * BLK][None]]
    dot_general x1 -> x0, matrix products: 10.5 us -> none  [body(): lax.dot_general(whole.reshape(seqs * n, whole.shape[2]), d_values.reshape...]
    concatenate x2 -> x0, other arithmetic: 8.14 us -> none  [the longest x1 7.41 us: body(): jnp.concatenate([gk[:slots].reshape(devices, CAP, BLK, ch), gv[:slots].re...]
  transfers between devices with their start and end apart: 4 -> 1, of which waited for: 3 -> 1; matrix products, arithmetic and copies ran while one was open for 3% -> 6% of each run, Pallas kernels for 3% -> 37%
where the time goes in v2:
time: 169 us; the launch traced here: 168 us
  Pallas kernels  119 us (70%)
  waiting for transfers between devices  15.9 us (9%)
  between operations  14.2 us (8%)
  local copies, waits for them, and re-layouts  9.46 us (6%)
  other arithmetic  9.13 us (5%)
    pallas_call x1, Pallas kernels, reduce_weight(): pl.pallas_call(reduce_kernel, in_specs=[whole] + [hbm] * 4, out_specs=[wh...  57.9 us
    pallas_call x1, Pallas kernels, gather_attention(): pl.pallas_call(gather_kernel, in_specs=[whole] * 3 + [hbm] * 5, out_specs...  48.6 us
    all_gather x1, waiting for transfers between devices, body(): whole = lax.all_gather(layer_input, 'tp', axis=0)  15.3 us
    pallas_call x1, Pallas kernels, remote_attention(): pl.pallas_call(remote_kernel, grid=(seqs,), in_specs=[pl.BlockSpec(memory...  12.7 us
  transfers between devices with their start and end apart: 1, of which 1 were waited for; matrix products, arithmetic and copies ran while one was open for 6% of the time, Pallas kernels for 37%

profile of v2, /device:TPU:0, one launch (start us, length us, event | category | flops | bytes accessed | tf_op | source)
XLA Modules:
  0.0 168.0 jit_solution(3127280715383339625)
XLA Ops:
  7.2 0.7 all-gather.3.cloned.1.call-update
  7.9 0.8 copy.14
  8.7 0.7 compare_and_fusion
  9.5 0.1 copy.16
  9.6 0.2 convert_reduce_fusion
  9.8 0.2 reshape.236
  10.0 0.1 broadcast_in_dim.60
  10.1 1.4 compare_reduce_fusion.1
  11.6 0.7 reshape.237.sel_ref
  12.4 0.7 pad.5.need
  13.0 1.4 multiply_bitcast_fusion.lse_ref
  14.4 48.6 %gather_attention.1 = (f32[4,512,512]{2,1,0:T(8,128)}, bf16[4,512,512]{2,1,0:T(8,128)(2,1)}, bf16[4,512,512]{2,1,0:T(8,128)(2,1)}, f32[4,4,512]{2,1,0:T(4,128)},...) custom-call(f32[2,4,4,8,128]{4,3,2,1,0:T(8,128)} %pad.5.need, ...), custom_call_target="tpu_custom_call" | custom-call | flops 20000000000 | bytes 31457280 | tf_op jit(solution)/shard_map/gather_attention/pallas_call | solution.py:293
  63.1 1.0 convert_reduce_fusion.1
  64.1 0.1 select_n.110
  64.2 0.1 compare_reduce_fusion
  64.5 0.1 broadcast_in_dim.70
  64.6 0.1 reshape.239
  64.7 0.8 broadcast_in_dim.71.sel_ref
  65.5 0.7 slice_convert_fusion
  66.7 0.5 broadcast_select_fusion.1.seq_ref
  67.2 12.7 %remote_attention.1 = (bf16[4,512,512]{2,1,0:T(8,128)(2,1)}, bf16[66,64,512]{2,1,0:T(8,128)(2,1)}, bf16[66,64,512]{2,1,0:T(8,128)(2,1)}) custom-call(s32[64]{0:T(128)} %broadcast_select_fusion.1.seq_ref, bf16[4,512,512]{2,1,0:T(8,128)(2,1)} %q_ref.1, bf16[4,512,512]{2,1,0:T(8,128)(2,1)} %do_ref.1, f32[4,4,512]{2,1,0:T(4,128)} %multiply_bitcast_fusion.lse_ref, ...), custom_call_target="tpu_custom_call" | custom-call | flops 10737418240 | bytes 29360128 | tf_op jit(solution)/shard_map/remote_attention/pallas_call | solution.py:592
  79.9 15.3 %all-gather.3.cloned.1.call-done = bf16[16,512,512]{2,1,0:T(8,128)(2,1)} async-done(((bf16[4,512,512]{2,1,0:T(8,128)(2,1)}), bf16[16,512,512]{2,1,0:T(8,128)(2,1)}) %all-gather.3.cloned.1.call-update) | async-done | bytes 8388624 | tf_op jit(solution)/shard_map/all_gather | solution.py:622
  95.2 57.9 %reduce_weight.1 = (f32[128,512]{1,0:T(8,128)}, f32[128,512]{1,0:T(8,128)}, f32[64,512]{1,0:T(8,128)}) custom-call(bf16[16,128]{1,0:T(8,128)(2,1)} %get-tuple-element.23.hot_ref, bf16[33,128,512]{2,1,0:T(8,128)(2,1)} %bitcast.44, bf16[33,128,512]{2,1,0:T(8,128)(2,1)} %bitcast.45, bf16[4,512,512]{2,1,0:T(8,128)(2,1)} %get-tuple-element.26.dv_hbm, ...), custom_call_target="tpu_custom_call" | custom-call | flops 20000000000 | bytes 20971520 | tf_op jit(solution)/shard_map/reduce_weight/pallas_call | solution.py:498
  153.1 1.1 fusion.14
  154.2 0.5 mul.135
  154.7 0.5 mul.128
  155.3 0.5 mul.141
  155.8 0.5 mul.138
  156.4 0.5 copy-done
  156.9 0.6 copy-done.1
  157.5 3.0 %fusion.1 = (bf16[4,512,512]{2,1,0:T(8,128)(2,1)}, bf16[4,512,512]{2,1,0:T(8,128)(2,1)}) fusion(bf16[4,512,512]{2,1,0:T(8,128)(2,1)S(1)} %copy-done.1, f32[4,512]{1,0:T(4,128)S(1)} %mul.133, f32[4,512]{1,0:T(4,128)S(1)} %mul.126, bf16[4,512,512]{2,1,0:T(8,128)(2,1)S(1)} %copy-done, f32[4,512,512]{2,1,0:T(8,128)S(1)} %bitcast.38, ...), kind=kLoop, calls=%fused_computation.2 | loop fusion | flops 12582912 | bytes 25182208 | tf_op jit(solution)/shard_map/convert_element_type | solution.py:662
  160.5 0.7 copy.20
  (26 shorter events, 0.9 us)
Async XLA Ops:
  7.2 88.0 %all-gather.3.cloned.1.call-start = ((), (), s32[]{:S(2)}) async-start(), calls=%async_computation | async-start | bytes 10485760 | tf_op jit(solution)/shard_map/all_gather | solution.py:622
  155.3 1.6 copy-start
  155.3 2.2 %copy-start.1 = (bf16[4,512,512]{2,1,0:T(8,128)(2,1)S(1)}, bf16[4,512,512]{2,1,0:T(8,128)(2,1)}, u32[]{:S(2)}) copy-start(bf16[4,512,512]{2,1,0:T(8,128)(2,1)} %get-tuple-element.26.dv_hbm) | copy-start | bytes 6291460
  157.5 3.0 %copy-start.2 = (f32[64,512]{1,0:T(8,128)S(1)}, f32[64,512]{1,0:T(8,128)}, u32[]{:S(2)}) copy-start(f32[64,512]{1,0:T(8,128)} %get-tuple-element.51) | copy-start | bytes 393220
Sparse Core Ops, SparseCore 0:
  9.6 85.5 all-gather.2

commit v3 on v1

v3 whole, which is shorter than its diff:
```python
import functools
import jax
import jax.numpy as jnp
from jax import lax
from jax.experimental import pallas as pl
from jax.experimental.pallas import tpu as pltpu
from jax.sharding import PartitionSpec as P

BLK = 64
CAP = 2
DH = 128
LOG2E = 1.4426950408889634
ROOT = DH ** -0.5
BIG = 1e30

NT = (((1,), (1,)), ((), ()))
TN = (((0,), (0,)), ((), ()))
NN = (((1,), (0,)), ((), ()))


def mm(a, b, dims):
    return lax.dot_general(a, b, dims, preferred_element_type=jnp.float32)


class Net:
    def __init__(self, send, recv):
        self.send, self.recv, self.n, self.all = send, recv, 0, []

    def copy(self, src, dst, kv, tp=None):
        i = self.n
        self.n += 1
        c = pltpu.make_async_remote_copy(
            src_ref=src, dst_ref=dst, send_sem=self.send.at[i], recv_sem=self.recv.at[i],
            device_id=(kv, lax.axis_index("tp") if tp is None else tp), device_id_type=pl.DeviceIdType.MESH)
        c.start()
        self.all.append(c)
        return c

    def finish(self):
        for c in self.all:
            c.wait_send()


class Disk:
    def __init__(self, sems):
        self.sems, self.n, self.all = sems, 0, []

    def copy(self, src, dst):
        c = pltpu.make_async_copy(src, dst, self.sems.at[self.n])
        self.n += 1
        c.start()
        return c

    def keep(self, src, dst):
        self.all.append(self.copy(src, dst))

    def finish(self):
        for c in self.all:
            c.wait()


def place():
    me = lax.axis_index("kv")
    return me // 8, (me // 2) % 4, me % 2


def kv_of(z, y, c):
    return (z * 4 + y) * 2 + c


def barrier_with(peers, across):
    sem = pltpu.get_barrier_semaphore()
    for kv in peers:
        pl.semaphore_signal(sem, inc=1, device_id=(kv, lax.axis_index("tp")),
                            device_id_type=pl.DeviceIdType.MESH)
    for tp in across:
        pl.semaphore_signal(sem, inc=1, device_id=(lax.axis_index("kv"), tp),
                            device_id_type=pl.DeviceIdType.MESH)
    pl.semaphore_wait(sem, len(peers) + len(across))


class Gather:
    def __init__(self, net, buf, y_first):
        z, y, c = place()
        self.net, self.buf, self.y_first = net, buf, y_first
        f, s = (y, z) if y_first else (z, y)
        self.c = c
        self.f = [f, (f + 3) % 4, (f + 1) % 4, (f + 2) % 4]
        self.s = [s, (s + 3) % 4, (s + 1) % 4, (s + 2) % 4]
        self.side, self.sent = [], []

    def full(self, f, s, c=None):
        c = self.c if c is None else c
        return self.buf.at[(c, s, f) if self.y_first else (c, f, s)]

    def half(self, f, s, which):
        c = self.c
        return self.buf.at[(c, s, f, which) if self.y_first else (c, f, s, which)]

    def send(self, ref, f, s, c=None):
        c = self.c if c is None else c
        x = self.net.copy(ref, ref, kv_of(s, f, c) if self.y_first else kv_of(f, s, c))
        self.sent.append(x)
        return x

    def have(self, f, s):
        self.side.append(self.send(self.full(f, s), self.f[0], self.s[0], 1 - self.c))

    def across(self, f):
        return (self.send(self.full(f, self.s[0]), self.f[0], self.s[2]),
                self.send(self.full(f, self.s[0]), self.f[0], self.s[1]))

    def phase0(self):
        own = self.full(self.f[0], self.s[0])
        self.a = self.send(own, self.f[2], self.s[0])
        self.b = self.send(own, self.f[1], self.s[0])
        self.second = [self.across(self.f[0])]
        self.have(self.f[0], self.s[0])

    def phase1(self):
        self.a.wait_recv()
        self.e = self.send(self.half(self.f[1], self.s[0], 0), self.f[2], self.s[0])
        self.second.append(self.across(self.f[1]))
        self.b.wait_recv()
        self.g = self.send(self.half(self.f[2], self.s[0], 1), self.f[1], self.s[0])
        self.second.append(self.across(self.f[2]))
        self.have(self.f[1], self.s[0])
        self.have(self.f[2], self.s[0])

    def phase2(self):
        self.e.wait_recv()
        self.g.wait_recv()
        self.second.append(self.across(self.f[3]))
        self.have(self.f[3], self.s[0])
        self.last = []

    def phase3(self, j):
        up, down = self.second[j]
        up.wait_recv()
        p = self.send(self.half(self.f[j], self.s[1], 0), self.f[0], self.s[2])
        down.wait_recv()
        q = self.send(self.half(self.f[j], self.s[2], 1), self.f[0], self.s[1])
        self.last.append((p, q))
        self.have(self.f[j], self.s[1])
        self.have(self.f[j], self.s[2])

    def phase4(self, j):
        for c in self.last[j]:
            c.wait_recv()
        self.have(self.f[j], self.s[3])

    def phase5(self):
        for c in self.side:
            c.wait_recv()

    def drain(self):
        for c in self.sent:
            c.wait_send()


class Route:
    def __init__(self, net, buf, rows, y_first, slots):
        z, y, c = place()
        self.net, self.buf, self.rows, self.y_first = net, buf, rows, y_first
        self.ra, self.rb, self.rp, self.rm, self.e, self.ta, self.tb, self.tp, self.tm = slots
        self.c = c
        self.f, self.s = (y, z) if y_first else (z, y)
        self.wide = buf.shape[-1] // 2
        self.kind = self.e.dtype

    def dev(self, f, s):
        return kv_of(s, f, self.c) if self.y_first else kv_of(f, s, self.c)

    def src(self, f, part=None):
        lanes = pl.ds(0, 2 * self.wide) if part is None else pl.ds(part * self.wide, self.wide)
        if self.y_first:
            return self.buf.at[:, f, self.rows, :, lanes]
        return self.buf.at[f, :, self.rows, :, lanes]

    def step1(self):
        f, s = self.f, self.s
        self.c1 = (self.net.copy(self.src((f + 2) % 4, 0), self.ra, self.dev((f + 1) % 4, s)),
                   self.net.copy(self.src((f + 2) % 4, 1), self.rb, self.dev((f + 3) % 4, s)))

    def step2(self):
        f, s, w = self.f, self.s, self.wide
        self.c2 = []
        for i, (d, got, dst) in enumerate(((1, self.ra, self.rp), (3, self.rb, self.rm))):
            self.c1[i].wait_recv()
            at = self.src((f + d) % 4, i)
            at[...] = (at[...].astype(jnp.float32) + got[...].astype(jnp.float32)).astype(jnp.bfloat16)
            self.c2.append(self.net.copy(self.src((f + d) % 4), dst, self.dev((f + d) % 4, s)))

    def step3(self):
        f, s, w = self.f, self.s, self.wide
        for x in self.c2:
            x.wait_recv()
        total = self.src(f)[...].astype(jnp.float32) + self.rp[...].astype(jnp.float32)
        self.e[...] = (total + self.rm[...].astype(jnp.float32)).astype(self.kind)
        far = (s + 2) % 4
        self.c3 = (self.net.copy(self.e.at[far, :, pl.ds(0, w)], self.ta, self.dev(f, (s + 1) % 4)),
                   self.net.copy(self.e.at[far, :, pl.ds(w, w)], self.tb, self.dev(f, (s + 3) % 4)))

    def step4(self):
        f, s, w = self.f, self.s, self.wide
        self.c4 = []
        for i, (d, got, dst) in enumerate(((1, self.ta, self.tp), (3, self.tb, self.tm))):
            self.c3[i].wait_recv()
            at = self.e.at[(s + d) % 4, :, pl.ds(i * w, w)]
            at[...] = (at[...].astype(jnp.float32) + got[...].astype(jnp.float32)).astype(self.kind)
            self.c4.append(self.net.copy(self.e.at[(s + d) % 4], dst, self.dev(f, (s + d) % 4)))

    def step5(self):
        for x in self.c4:
            x.wait_recv()
        total = self.e[self.s].astype(jnp.float32) + self.tp[...].astype(jnp.float32)
        return total + self.tm[...].astype(jnp.float32)


def route_scratch(rows, ch, kind):
    bf = jnp.bfloat16
    return [pltpu.VMEM((4, rows, ch // 2), bf), pltpu.VMEM((4, rows, ch // 2), bf),
            pltpu.VMEM((4, rows, ch), bf), pltpu.VMEM((4, rows, ch), bf), pltpu.VMEM((4, rows, ch), kind),
            pltpu.VMEM((rows, ch // 2), kind), pltpu.VMEM((rows, ch // 2), kind),
            pltpu.VMEM((rows, ch), kind), pltpu.VMEM((rows, ch), kind)]


class Stream:
    def __init__(self, net, buf, slots):
        self.routes = [Route(net, buf, 0, True, slots[:9]), Route(net, buf, 1, False, slots[9:])]

    def run(self, name):
        return [getattr(r, name)() for r in self.routes]


class Ring:
    def __init__(self, net, own, everyone):
        self.net, self.own, self.all = net, own, everyone
        t = lax.axis_index("tp")
        self.t = [t, (t + 3) % 4, (t + 1) % 4, (t + 2) % 4]
        self.onward = []

    def start(self):
        t = self.t
        self.up, self.down = [], []
        for j in range(4):
            self.up.append(self.copy(self.own.at[j], self.all.at[t[0], j], t[2]))
            i = (j + 2) % 4
            self.down.append(self.copy(self.own.at[i], self.all.at[t[0], i], t[1]))

    def copy(self, src, dst, tp):
        return self.net.copy(src, dst, lax.axis_index("kv"), tp)

    def pass_on(self, j):
        self.up[j].wait_recv()
        at = self.all.at[self.t[1], j]
        self.onward.append(self.copy(at, at, self.t[2]))
        self.down[j].wait_recv()
        at = self.all.at[self.t[2], j + 2]
        self.onward.append(self.copy(at, at, self.t[1]))

    def near(self):
        for c in self.up[2:] + self.down[2:]:
            c.wait_recv()

    def far(self):
        for c in self.onward:
            c.wait_recv()


def whole_kernel(code_ref, lse_ref, pick_ref, q_hbm, k_hbm, v_hbm, o_hbm, do_hbm, x_hbm,
                 dq_hbm, dk_hbm, dv_hbm, dw_ref, xall_hbm,
                 qb, kb, vb, ob, dob, dqt, dkb, dvb, dqb, delta_ref,
                 need, rc, n1, ry, n2, rz, tab, pka, pva, pkb, pvb, gk, gv, part,
                 info, spots, info_s, spots_s, to_s, rka, rva, rkb, rvb, ws, wr, wb, *rest):
    kas, vas, kbs, vbs, wslots = (rest[i * 18:i * 18 + 18] for i in range(5))
    send, recv, local = rest[90:]
    z, y, c = place()
    me = lax.axis_index("kv")
    net, disk = Net(send, recv), Disk(local)
    loads = [disk.copy(a, b) for a, b in
             ((k_hbm, kb), (v_hbm, vb), (q_hbm, qb), (do_hbm, dob), (o_hbm, ob))]
    partner = kv_of(z, y, 1 - c)
    peers = [partner]
    for d in range(1, 4):
        peers += [kv_of(z, (y + d) % 4, c), kv_of((z + d) % 4, y, c)]
    x = Ring(net, x_hbm, xall_hbm)
    barrier_with(peers, x.t[1:3])

    seqs, n, ch = qb.shape
    half = n // 2

    def six(ref):
        return ref.reshape(2, 4, 4, CAP, BLK, ch // 2)

    blocks = n // BLK
    wide = ch // 2
    slots = 32 * CAP
    room = 18

    flat = (lax.broadcasted_iota(jnp.int32, (32, 128), 0) * 128 +
            lax.broadcasted_iota(jnp.int32, (32, 128), 1))

    def mark(i, seen):
        for j in range(8):
            seen = jnp.where(flat == code_ref[i * 8 + j], 1, seen)
        return seen

    seen = lax.fori_loop(0, code_ref.shape[0] // 8, mark, jnp.zeros((32, 128), jnp.int32))
    for i in range(32):
        need[i // 16, i // 4 % 4, i % 4] = jnp.broadcast_to(seen[i:i + 1], (8, 128))
    first = net.copy(need.at[1 - c], rc, partner)
    x.start()
    for l in loads:
        l.wait()

    def bias_row(lse, s, block):
        hit = jnp.max(jnp.where(pick_ref[s] == block, 1, 0), axis=0, keepdims=True)
        return jnp.where(hit > 0, lse, BIG)

    def unit(u, _):
        s = u // 2
        for g in range(2):
            h = (u % 2) * 2 + g
            hs = pl.ds(pl.multiple_of(h * DH, DH), DH)
            hr = pl.ds(h, 1)
            q = qb[s, :, hs]
            do = dob[s, :, hs]
            prod = do.astype(jnp.float32) * ob[s, :, :, hs].reshape(n, DH).astype(jnp.float32)
            delta = jnp.sum(prod.T, axis=0, keepdims=True)
            delta_ref[s, hr, :] = delta
            lse = lse_ref[s, hr, :]
            parts = []
            for t in range(2):
                lo = t * half
                here = slice(lo // BLK, (lo + half) // BLK)
                k = kb[s, here, :, hs].reshape(half, DH)
                v = vb[s, here, :, hs].reshape(half, DH)
                qc, doc = q[lo:], do[lo:]
                w = n - lo
                sc = mm(k, qc, NT)
                row = lax.broadcasted_iota(jnp.int32, (half, w), 0)
                col = lax.broadcasted_iota(jnp.int32, (half, w), 1)
                bias = jnp.concatenate(
                    [jnp.broadcast_to(bias_row(lse, s, me * blocks + j)[:, lo:], (BLK, w))
                     for j in range(lo // BLK, (lo + half) // BLK)], axis=0)
                p = jnp.exp2(jnp.where(row <= col, sc * (ROOT * LOG2E) - bias, -BIG))
                dp = mm(v, doc, NT)
                ds = (p * (dp - delta[:, lo:])).astype(jnp.bfloat16)
                dvb[s, here, :, hs] = mm(p.astype(jnp.bfloat16), doc, NN).astype(jnp.bfloat16).reshape(-1, BLK, DH)
                dkb[s, here, :, hs] = (mm(ds, qc, NN) * ROOT).astype(jnp.bfloat16).reshape(-1, BLK, DH)
                parts.append(mm(k, ds, TN))
            dqt[s, hs, :half] = parts[0][:, :half]
            dqt[s, hs, half:] = parts[0][:, half:] + parts[1]
        return 0

    def units(a, b):
        lax.fori_loop(a, b, unit, 0)

    units(0, 1)
    first.wait_recv()
    n1[...] = jnp.maximum(need[c], rc[...])
    ys = [net.copy(n1.at[(y + d) % 4], ry.at[d - 1], kv_of(z, (y + d) % 4, c)) for d in range(1, 4)]
    units(1, 2)
    for a in ys:
        a.wait_recv()
    n2[...] = jnp.maximum(jnp.maximum(n1[y], ry[0]), jnp.maximum(ry[1], ry[2]))
    zs = [net.copy(n2.at[(z + d) % 4], rz.at[d - 1], kv_of((z + d) % 4, y, c)) for d in range(1, 4)]
    units(2, 3)
    for a in zs:
        a.wait_recv()
    need1 = jnp.maximum(jnp.maximum(n2[z], rz[0]), jnp.maximum(rz[1], rz[2]))
    info[...] = need1
    disk.copy(info, info_s).wait()

    def first_two(i, state):
        seen, s0, s1 = state
        here = info_s[0, i]
        s0 = jnp.where((here == 1) & (seen == 0), i, s0)
        s1 = jnp.where((here == 1) & (seen == 1), i, s1)
        return seen + here, s0, s1

    minus = jnp.int32(-1)
    _, served0, served1 = lax.fori_loop(0, seqs * blocks, first_two, (jnp.int32(0), minus, minus))
    served = (served0, served1)
    lane8 = lax.broadcasted_iota(jnp.int32, (8, 128), 1)
    tab[c, z, y] = jnp.where(lane8 == 0, served0, jnp.where(lane8 == 1, served1, minus))
    tys = [net.copy(tab.at[c, z, y], tab.at[c, z, y], kv_of(z, (y + d) % 4, c)) for d in range(1, 4)]

    def rows_of(ref):
        out = []
        for b in served:
            b = jnp.clip(b, 0, seqs * blocks - 1)
            out.append(ref[b // blocks, b % blocks])
        return out

    for b, (pick_k, pick_v) in enumerate(zip(rows_of(kb), rows_of(vb))):
        at = (c * 16 + z * 4 + y) * CAP + b
        pka[at] = pick_k[:, :wide]
        pva[at] = pick_v[:, :wide]
        pkb[at] = pick_k[:, wide:]
        pvb[at] = pick_v[:, wide:]

    ga = [Gather(net, six(pka), True), Gather(net, six(pva), False)]
    gb = [Gather(net, six(pkb), True), Gather(net, six(pvb), False)]

    def each(gs, name, *j):
        for g in gs:
            getattr(g, name)(*j)

    each(ga, "phase0")
    units(3, 5)
    for a in tys:
        a.wait_recv()
    tzs = [net.copy(tab.at[c, z], tab.at[c, z], kv_of((z + d) % 4, y, c)) for d in range(1, 4)]
    each(ga, "phase1")
    units(5, 6)
    each(ga, "phase2")
    each(gb, "phase0")
    for a in tzs:
        a.wait_recv()
    tside = net.copy(tab.at[c], tab.at[c], partner)
    units(6, 7)
    each(ga, "phase3", 0)
    each(ga, "phase3", 1)
    each(gb, "phase1")
    units(7, 8)
    own_x = disk.copy(x_hbm, kb)
    tside.wait_recv()
    for i in range(32):
        spots[i:i + 1] = tab[i // 16, i // 4 % 4, i % 4, 0:1]
    disk.copy(spots, spots_s).wait()

    def owner_of(p):
        o = p // CAP
        return o, o % 16 * 2 + o // 16

    def tally(p, sums):
        o, kvi = owner_of(p)
        v = spots_s[o, p % CAP]
        live = (v >= 0) & (kvi < me)
        return tuple(t + jnp.where(live & (v // blocks == s), 1, 0) for s, t in enumerate(sums))

    zero = jnp.int32(0)
    sums = lax.fori_loop(0, slots, tally, (zero,) * 4)
    chunks = [(t + 3) // 4 for t in sums]
    base = [zero]
    for s in range(3):
        base.append(base[-1] + chunks[s])

    def arrange(p, state):
        heads_at, l_slot, l_id = state
        o, kvi = owner_of(p)
        v = spots_s[o, p % CAP]
        live = (v >= 0) & (kvi < me)
        to = jnp.int32(4 * room)
        now = []
        for s, t in enumerate(heads_at):
            hit = live & (v // blocks == s)
            to = jnp.where(hit, t, to)
            now.append(t + jnp.where(hit, 1, 0))
        to_s[0, p] = to
        here = lane8 == to
        return tuple(now), jnp.where(here, p, l_slot), jnp.where(here, kvi * blocks + v % blocks, l_id)

    blank = jnp.zeros((8, 128), jnp.int32)
    _, l_slot, l_id = lax.fori_loop(
        0, slots, arrange, (tuple(4 * b for b in base), blank, blank - 5))
    row8 = lax.broadcasted_iota(jnp.int32, (8, 128), 0)
    info[...] = jnp.where(row8 == 0, l_slot, l_id)
    to_info = disk.copy(info, info_s)
    gk[4 * room] = jnp.zeros(gk.shape[1:], gk.dtype)
    gv[4 * room] = jnp.zeros(gv.shape[1:], gv.dtype)
    to_info.wait()
    count_me = jnp.where(me == 0, 0, (2 * me + 12) // 4)

    def seq_of(i):
        return sum(jnp.where(i >= base[s], 1, 0) for s in range(1, 4))

    each(ga, "phase3", 2)
    each(ga, "phase3", 3)
    each(gb, "phase2")
    for j in range(4):
        each(ga, "phase4", j)
    each(ga, "phase5")

    def attend(second):
        pk, pv = (pkb, pvb) if second else (pka, pva)

        def chunk(i, _):
            s = seq_of(i)
            keep = jnp.where((s == seq_of(i - 1)) & (i > 0), 1, 0)
            keep = jnp.broadcast_to(keep, (1, n)) == 1
            who = [(jnp.clip(info_s[0, 4 * i + e], 0, slots - 1), info_s[1, 4 * i + e]) for e in range(4)]
            for g in range(2):
                h = 2 * second + g
                gs = slice(g * DH, (g + 1) * DH)
                hs = slice(h * DH, (h + 1) * DH)
                q = qb[s, :, hs]
                do = dob[s, :, hs]
                k = jnp.concatenate([pk[o, :, gs] for o, _ in who], axis=0)
                v = jnp.concatenate([pv[o, :, gs] for o, _ in who], axis=0)
                lse = lse_ref[s, h:h + 1, :]
                st = mm(k, q, NT)
                bias = jnp.concatenate(
                    [jnp.broadcast_to(bias_row(lse, s, b), (BLK, n)) for _, b in who], axis=0)
                p = jnp.exp2(st * (ROOT * LOG2E) - bias)
                dp = mm(v, do, NT)
                ds = (p * (dp - delta_ref[s, h:h + 1, :])).astype(jnp.bfloat16)
                dv = mm(p.astype(jnp.bfloat16), do, NN).astype(jnp.bfloat16)
                dk = (mm(ds, q, NN) * ROOT).astype(jnp.bfloat16)
                for e in range(4):
                    gv[4 * i + e, :, gs] = dv[e * BLK:(e + 1) * BLK]
                    gk[4 * i + e, :, gs] = dk[e * BLK:(e + 1) * BLK]
                old = part[2 * jnp.maximum(i - 1, 0) + g]
                part[2 * i + g] = jnp.where(keep, old, 0.0) + mm(k, ds, TN)
            return 0

        return lambda a, b: lax.fori_loop(jnp.minimum(a, count_me), jnp.minimum(b, count_me), chunk, 0)

    def settle(second):
        pk, pv = (pkb, pvb) if second else (pka, pva)

        def move(o, _):
            for b in range(CAP):
                to = jnp.clip(to_s[0, o * CAP + b], 0, 4 * room)
                pk[o * CAP + b] = gk[to]
                pv[o * CAP + b] = gv[to]
            return 0

        lax.fori_loop(0, 32, move, 0)

    def queries(second):
        for s in range(seqs):
            end = jnp.clip(base[s] + chunks[s] - 1, 0, room - 1)
            for g in range(2):
                h = 2 * second + g
                hs = slice(h * DH, (h + 1) * DH)
                more = jnp.where(jnp.broadcast_to(chunks[s], (1, n)) > 0, part[2 * end + g], 0.0)
                dqb[s, :, :, hs] = ((dqt[s, hs, :] + more).T * ROOT).astype(jnp.bfloat16).reshape(-1, BLK, DH)

    def side(buf, into):
        return net.copy(six(buf).at[1 - c], into, partner)

    def fold(buf, into, copy):
        copy.wait_recv()

        def add(i, _):
            at = c * 32 + i
            a = buf[at].astype(jnp.float32)
            buf[at] = (a + into[i // 8, i // 2 % 4, i % 2].astype(jnp.float32)).astype(jnp.bfloat16)
            return 0

        lax.fori_loop(0, 32, add, 0)

    first_half = attend(0)
    first_half(0, 3)
    each(gb, "phase3", 0)
    each(gb, "phase3", 1)
    first_half(3, 6)
    each(gb, "phase3", 2)
    each(gb, "phase3", 3)
    first_half(6, 9)
    for j in range(4):
        each(gb, "phase4", j)
    x.pass_on(0)
    first_half(9, room)
    each(gb, "phase5")
    each(ga, "drain")
    settle(0)
    side_va = side(pva, rva)
    side_ka = side(pka, rka)
    queries(0)
    va = Stream(net, six(pva).at[c], vas)
    ka = Stream(net, six(pka).at[c], kas)
    second_half = attend(1)
    fold(pva, rva, side_va)
    va.run("step1")
    second_half(0, 2)
    fold(pka, rka, side_ka)
    ka.run("step1")
    second_half(2, 6)
    va.run("step2")
    x.pass_on(1)
    second_half(6, 10)
    ka.run("step2")
    second_half(10, 14)
    va.run("step3")
    second_half(14, room)
    each(gb, "drain")
    settle(1)
    side_vb = side(pvb, rvb)
    side_kb = side(pkb, rkb)
    va.run("step4")
    ka.run("step3")
    queries(1)
    dq_out = disk.copy(dqb, dq_hbm)
    vsb = Stream(net, six(pvb).at[c], vbs)
    ksb = Stream(net, six(pkb).at[c], kbs)
    fold(pvb, rvb, side_vb)
    vsb.run("step1")
    fold(pkb, rkb, side_kb)
    ksb.run("step1")
    ka.run("step4")

    x.near()
    load_x = [own_x, disk.copy(xall_hbm.at[x.t[1]], vb), disk.copy(xall_hbm.at[x.t[2]], ob)]
    bufs = [kb, vb, ob, dqb]

    def product(i):
        load_x[i].wait()

        def step(s, _):
            r = mm(bufs[i][s].reshape(n, ch), dvb[s].reshape(n, ch), TN)
            for j in range(4):
                at = x.t[i] * 4 + j
                part[at] = part[at] + r[j * 128:(j + 1) * 128]
            return 0

        r = mm(bufs[i][0].reshape(n, ch), dvb[0].reshape(n, ch), TN)
        for j in range(4):
            part[x.t[i] * 4 + j] = r[j * 128:(j + 1) * 128]
        lax.fori_loop(1, seqs, step, 0)

    product(0)
    vsb.run("step2")
    fva = va.run("step5")
    product(1)
    ksb.run("step2")
    fka = ka.run("step5")
    vsb.run("step3")
    product(2)
    vsb.run("step4")
    x.far()
    dq_out.wait()
    load_x.append(disk.copy(xall_hbm.at[x.t[3]], dqb))
    product(3)
    old = jnp.concatenate(rows_of(dvb), axis=0).astype(jnp.float32)
    xs = [jnp.concatenate(rows_of(b), axis=0) for b in bufs]
    fvb = vsb.run("step5")

    def joined(a, b):
        return jnp.concatenate([jnp.concatenate(a, axis=0), jnp.concatenate(b, axis=0)], axis=1)

    extra_v = joined(fva, fvb)
    diff = ((old + extra_v).astype(jnp.bfloat16).astype(jnp.float32) - old).astype(jnp.bfloat16)
    mine, other = pl.multiple_of(c * BLK, BLK), pl.multiple_of((1 - c) * BLK, BLK)
    for i in range(4):
        r = mm(xs[i], diff, TN)
        for j in range(4):
            at = x.t[i] * 4 + j
            part[at] = part[at] + r[j * 128:(j + 1) * 128]
            ws[at] = part[at, pl.ds(other, BLK)].astype(jnp.bfloat16)
    side_w = net.copy(ws, wr, partner)
    ksb.run("step3")
    side_w.wait_recv()
    for i in range(16):
        own = part[i, pl.ds(mine, BLK)]
        wb[i // 4, i % 4] = (own + wr[i].astype(jnp.float32)).astype(jnp.bfloat16).reshape(2, BLK // 2, ch)
    w = Stream(net, wb, wslots)
    w.run("step1")
    ksb.run("step4")

    def finish(local_ref, extra):
        def add(i, _):
            at = (i // blocks, i % blocks)
            more = jnp.where(served0 == i, extra[:BLK], 0.0) + jnp.where(served1 == i, extra[BLK:], 0.0)
            local_ref[at] = (local_ref[at].astype(jnp.float32) + more).astype(jnp.bfloat16)
            return 0

        lax.fori_loop(0, seqs * blocks, add, 0)

    w.run("step2")
    finish(dvb, extra_v)
    disk.keep(dvb, dv_hbm)
    fkb = ksb.run("step5")
    w.run("step3")
    finish(dkb, joined(fka, fkb))
    disk.keep(dkb, dk_hbm)
    w.run("step4")
    top, low = w.run("step5")
    dw_ref[:BLK // 2] = top
    dw_ref[BLK // 2:] = low
    done = set(id(a) for g in ga + gb for a in g.sent)
    for a in net.all:
        if id(a) not in done:
            a.wait_send()
    disk.finish()


def fused(code, lse, pick, q, k, v, o, do, x):
    seqs, n, ch = q.shape
    blk = k.shape
    heads = ch // DH
    bf, f32, i32 = jnp.bfloat16, jnp.float32, jnp.int32
    wide = ch // 2
    whole = pl.BlockSpec(memory_space=pltpu.VMEM)
    hbm = pl.BlockSpec(memory_space=pl.ANY)
    V = pltpu.VMEM
    return pl.pallas_call(
        whole_kernel,
        in_specs=[pl.BlockSpec(memory_space=pltpu.SMEM)] + [whole] * 2 + [hbm] * 6,
        out_specs=[hbm] * 3 + [whole, hbm],
        out_shape=[
            jax.ShapeDtypeStruct(blk, bf),
            jax.ShapeDtypeStruct(blk, bf),
            jax.ShapeDtypeStruct(blk, bf),
            jax.ShapeDtypeStruct((BLK, ch), f32),
            jax.ShapeDtypeStruct((4,) + x.shape, bf),
        ],
        scratch_shapes=[V(q.shape, bf)] + [V(blk, bf)] * 3 + [V(q.shape, bf), V((seqs, ch, n), f32)] + [V(blk, bf)] * 3 + [
            V((seqs, heads, n), f32),
            V((2, 4, 4, 8, 128), i32), V((4, 4, 8, 128), i32), V((4, 4, 8, 128), i32),
            V((3, 4, 8, 128), i32), V((4, 8, 128), i32), V((3, 8, 128), i32), V((2, 4, 4, 8, 128), i32),
            V((64, BLK, wide), bf), V((64, BLK, wide), bf), V((64, BLK, wide), bf), V((64, BLK, wide), bf),
            V((73, BLK, wide), bf), V((73, BLK, wide), bf), V((36, DH, n), f32),
            V((8, 128), i32), V((32, 128), i32),
            pltpu.SMEM((8, 128), i32), pltpu.SMEM((32, 128), i32), pltpu.SMEM((8, 128), i32),
        ] + [V((4, 4, CAP, BLK, wide), bf)] * 4 + [
            V((16, BLK, ch), bf), V((16, BLK, ch), bf), V((4, 4, 2, BLK // 2, ch), bf),
        ] + (route_scratch(BLK, wide, bf) * 2 + route_scratch(BLK, wide, f32) * 2) * 2
        + route_scratch(BLK // 2, ch, f32) * 2 + [
            pltpu.SemaphoreType.DMA((256,)), pltpu.SemaphoreType.DMA((256,)), pltpu.SemaphoreType.DMA((20,)),
        ],
        compiler_params=pltpu.CompilerParams(
            vmem_limit_bytes=67043328, collective_id=0, has_side_effects=True),
        cost_estimate=pl.CostEstimate(flops=20_000_000_000, bytes_accessed=30 << 20, transcendentals=1 << 22),
        name="fused_backward",
    )(code, lse, pick, q, k, v, o, do, x)


def body(layer_input, queries, keys, values, outputs, d_out, log_sums, chosen):
    seqs, n, ch = queries.shape
    blocks = n // BLK
    me = lax.axis_index("kv")
    lse = jnp.swapaxes(log_sums, 1, 2) * LOG2E
    owner = chosen // blocks
    row = (owner % 2) * 16 + (owner // 2 % 4) * 4 + owner // 8
    lane = jnp.arange(seqs, dtype=jnp.int32)[:, None, None] * blocks + chosen % blocks
    code = jnp.where((chosen >= 0) & (owner != me), row * 128 + lane, -1).reshape(-1)
    pick = jnp.swapaxes(chosen, 1, 2)
    pick = jnp.pad(pick, ((0, 0), (0, 16 - pick.shape[1]), (0, 0)), constant_values=-1)
    pick = jnp.repeat(pick, BLK, axis=2)

    def cut(a):
        return a.reshape(seqs, blocks, BLK, ch)

    dq, dk, dv, dw, _ = fused(code, lse, pick, queries, cut(keys), cut(values), cut(outputs), d_out, cut(layer_input))
    return dq.reshape(queries.shape), dk.reshape(queries.shape), dv.reshape(queries.shape), dw


def solution(mesh):
    spec = P(None, "kv", "tp")
    return jax.shard_map(
        body,
        mesh=mesh,
        in_specs=(spec,) * 7 + (P(None, "kv", None),),
        out_specs=(spec, spec, spec, P("kv", "tp")),
        check_vma=False,
    )
```

time: 353 us -> 141 us (0.40)
  waiting for transfers between devices: 230 us -> 0 us
  Pallas kernels: 24.5 us -> 128 us
  blocking collectives: 26.4 us -> 0 us
  local copies, waits for them, and re-layouts: 30.7 us -> 9.93 us
  between operations: 15.4 us -> 0.67 us
  other arithmetic: 15.3 us -> 2.18 us
  matrix products: 10.5 us -> 0 us
    reduce_scatter x1 -> x0, waiting for transfers between devices: 112 us -> none  [body(): back = lax.psum_scatter(back, 'kv', scatter_dimension=0).astype(jnp.float32)]
    pallas_call x2 -> x1, Pallas kernels: 24.5 us -> 128 us  [fused(): pl.pallas_call(whole_kernel, in_specs=[pl.BlockSpec(memory_space=pltpu.SM...]
    unnamed x5 -> x0, waiting for transfers between devices: 82.4 us -> none
    all_gather x2 -> x0, waiting for transfers between devices: 35.1 us -> none  [the longest x1 35.1 us: body(): pool = lax.all_gather(sent, 'kv', axis=0)]
    all_gather x1 -> x0, blocking collectives: 26.4 us -> none  [body(): everyone = lax.all_gather(needed, 'kv').max(axis=0)]
    slice x4 -> x0, local copies, waits for them, and re-layouts: 13.2 us -> none  [the longest x1 5.98 us: body(): pv = pool[:, CAP:].reshape(devices * CAP, BLK, ch)]
    dot_general x1 -> x0, matrix products: 10.5 us -> none  [body(): lax.dot_general(whole.reshape(seqs * n, whole.shape[2]), d_values.reshape...]
    concatenate x2 -> x0, other arithmetic: 8.14 us -> none  [the longest x1 7.41 us: body(): jnp.concatenate([gk[:slots].reshape(devices, CAP, BLK, ch), gv[:slots].re...]
  transfers between devices with their start and end apart: 4 -> 0, of which waited for: 3 -> 0; matrix products, arithmetic and copies ran while one was open for 3% -> 0% of each run, Pallas kernels for 3% -> 0%
where the time goes in v3:
time: 141 us
  Pallas kernels  128 us (91%)
  local copies, waits for them, and re-layouts  9.93 us (7%)
  other arithmetic  2.18 us (2%)
    pallas_call x1, Pallas kernels, fused(): pl.pallas_call(whole_kernel, in_specs=[pl.BlockSpec(memory_space=pltpu.SM...  128 us
    unnamed x11, local copies, waits for them, and re-layouts  8.34 us

profile of v3, /device:TPU:0, one launch (start us, length us, event | category | flops | bytes accessed | tf_op | source)
XLA Modules:
  0.0 140.9 jit_solution(16345621559922810894)
XLA Ops:
  0.6 0.8 fusion.5
  1.4 0.7 reshape.40.code_ref
  2.1 1.4 multiply_bitcast_fusion.lse_ref
  3.5 0.8 copy.13
  4.3 0.1 broadcast_in_dim.6
  4.5 0.8 reshape.41.pick_ref
  5.2 128.1 %fused_backward.1 = (bf16[4,8,64,512]{3,2,1,0:T(8,128)(2,1)}, bf16[4,8,64,512]{3,2,1,0:T(8,128)(2,1)}, bf16[4,8,64,512]{3,2,1,0:T(8,128)(2,1)}, f32[64,512]{1,0:T(8,128)}, bf16[4,4,8,64,512]{4,3,2,1,0:T(8,128)(2,1)}) custom-call(s32[384]{0:T(512)} %reshape.40.code_ref, f32[4,4,512]{2,1,0:T(4,128)} %multiply_bitcast_fusion.lse_ref, ...), custom_call_target="tpu_custom_call" | custom-call | flops 20000000000 | bytes 31457280 | tf_op jit(solution)/shard_map/fused_backward/pallas_call | solution.py:700
  133.4 0.0 copy-start.1
  133.4 3.2 %copy.18 = bf16[4,512,512]{2,1,0:T(8,128)(2,1)} copy(bf16[4,512,512]{2,1,0:T(8,128)(2,1)} %bitcast.14) | data formatting | bytes 4194304
  136.6 0.0 copy-done.1
  136.6 0.0 copy-start
  136.6 1.3 copy.19
  137.9 1.0 copy-done
  139.0 0.0 copy-start.2
  139.0 1.3 copy.20
  140.3 0.0 copy-done.2
  140.3 0.7 copy.21
  (2 shorter events, 0.0 us)
Async XLA Ops:
  133.4 3.2 %copy-start.1 = (bf16[4,8,64,512]{3,2,1,0:T(8,128)(2,1)S(1)}, bf16[4,8,64,512]{3,2,1,0:T(8,128)(2,1)}, u32[]{:S(2)}) copy-start(bf16[4,8,64,512]{3,2,1,0:T(8,128)(2,1)} %get-tuple-element.9) | copy-start | bytes 6291460
  136.6 2.3 %copy-start = (bf16[4,8,64,512]{3,2,1,0:T(8,128)(2,1)S(1)}, bf16[4,8,64,512]{3,2,1,0:T(8,128)(2,1)}, u32[]{:S(2)}) copy-start(bf16[4,8,64,512]{3,2,1,0:T(8,128)(2,1)} %get-tuple-element.10) | copy-start | bytes 6291460
  139.0 1.3 copy-start.2

commit v4 on v3

--- a/solution.py
+++ b/solution.py
@@ -24,17 +24,36 @@
 
 class Net:
     def __init__(self, send, recv):
-        self.send, self.recv, self.n, self.all = send, recv, 0, []
-
-    def copy(self, src, dst, kv, tp=None):
-        i = self.n
+        self.send, self.recv, self.n, self.ns, self.all = send, recv, 0, 0, []
+
+    def new_send(self):
+        self.ns += 1
+        return self.ns - 1
+
+    def new_recv(self):
         self.n += 1
-        c = pltpu.make_async_remote_copy(
-            src_ref=src, dst_ref=dst, send_sem=self.send.at[i], recv_sem=self.recv.at[i],
+        return self.n - 1
+
+    def copy(self, src, dst, kv, tp=None, ss=None, rs=None):
+        shared = ss is not None
+        ss = self.new_send() if ss is None else ss
+        rs = self.new_recv() if rs is None else rs
+        c = self.make(src, dst, kv, tp, ss, rs)
+        c.start()
+        if not shared:
+            self.all.append(c)
+        return c
+
+    def make(self, src, dst, kv, tp, ss, rs):
+        return pltpu.make_async_remote_copy(
+            src_ref=src, dst_ref=dst, send_sem=self.send.at[ss], recv_sem=self.recv.at[rs],
             device_id=(kv, lax.axis_index("tp") if tp is None else tp), device_id_type=pl.DeviceIdType.MESH)
-        c.start()
-        self.all.append(c)
-        return c
+
+    def wait_recv(self, ref, rs):
+        self.make(ref, ref, (lax.axis_index("kv") + 1) % 32, None, 0, rs).wait_recv()
+
+    def wait_send(self, ref, ss):
+        self.make(ref, ref, (lax.axis_index("kv") + 1) % 32, None, ss, 0).wait_send()
 
     def finish(self):
         for c in self.all:
@@ -68,7 +87,7 @@
     return (z * 4 + y) * 2 + c
 
 
-def barrier_with(peers, across):
+def greet(peers, across):
     sem = pltpu.get_barrier_semaphore()
     for kv in peers:
         pl.semaphore_signal(sem, inc=1, device_id=(kv, lax.axis_index("tp")),
@@ -76,7 +95,9 @@
     for tp in across:
         pl.semaphore_signal(sem, inc=1, device_id=(lax.axis_index("kv"), tp),
                             device_id_type=pl.DeviceIdType.MESH)
-    pl.semaphore_wait(sem, len(peers) + len(across))
+
+
+SENDS, RECVS = 38, 189
 
 
 class Gather:
@@ -87,7 +108,7 @@
         self.c = c
         self.f = [f, (f + 3) % 4, (f + 1) % 4, (f + 2) % 4]
         self.s = [s, (s + 3) % 4, (s + 1) % 4, (s + 2) % 4]
-        self.side, self.sent = [], []
+        self.out, self.away, self.near = net.new_send(), net.new_send(), net.new_recv()
 
     def full(self, f, s, c=None):
         c = self.c if c is None else c
@@ -97,14 +118,15 @@
         c = self.c
         return self.buf.at[(c, s, f, which) if self.y_first else (c, f, s, which)]
 
-    def send(self, ref, f, s, c=None):
+    def send(self, ref, f, s, c=None, near=False):
         c = self.c if c is None else c
-        x = self.net.copy(ref, ref, kv_of(s, f, c) if self.y_first else kv_of(f, s, c))
-        self.sent.append(x)
-        return x
+        kv = kv_of(s, f, c) if self.y_first else kv_of(f, s, c)
+        if near:
+            return self.net.copy(ref, ref, kv, ss=self.away, rs=self.near)
+        return self.net.copy(ref, ref, kv, ss=self.out)
 
     def have(self, f, s):
-        self.side.append(self.send(self.full(f, s), self.f[0], self.s[0], 1 - self.c))
+        self.send(self.full(f, s), self.f[0], self.s[0], 1 - self.c, True)
 
     def across(self, f):
         return (self.send(self.full(f, self.s[0]), self.f[0], self.s[2]),
@@ -150,18 +172,17 @@
         self.have(self.f[j], self.s[3])
 
     def phase5(self):
-        for c in self.side:
-            c.wait_recv()
-
-    def drain(self):
-        for c in self.sent:
-            c.wait_send()
+        self.net.wait_recv(self.buf.at[1 - self.c], self.near)
+
+    def drain(self, flat):
+        self.net.wait_send(self.buf.at[self.c], self.away)
+        self.net.wait_send(flat.at[pl.ds(0, 30)], self.out)
 
 
 class Route:
-    def __init__(self, net, buf, rows, y_first, slots):
+    def __init__(self, net, buf, rows, y_first, slots, out):
         z, y, c = place()
-        self.net, self.buf, self.rows, self.y_first = net, buf, rows, y_first
+        self.net, self.buf, self.rows, self.y_first, self.out = net, buf, rows, y_first, out
         self.ra, self.rb, self.rp, self.rm, self.e, self.ta, self.tb, self.tp, self.tm = slots
         self.c = c
         self.f, self.s = (y, z) if y_first else (z, y)
@@ -179,8 +200,8 @@
 
     def step1(self):
         f, s = self.f, self.s
-        self.c1 = (self.net.copy(self.src((f + 2) % 4, 0), self.ra, self.dev((f + 1) % 4, s)),
-                   self.net.copy(self.src((f + 2) % 4, 1), self.rb, self.dev((f + 3) % 4, s)))
+        self.c1 = (self.net.copy(self.src((f + 2) % 4, 0), self.ra, self.dev((f + 1) % 4, s), ss=self.out),
+                   self.net.copy(self.src((f + 2) % 4, 1), self.rb, self.dev((f + 3) % 4, s), ss=self.out))
 
     def step2(self):
         f, s, w = self.f, self.s, self.wide
@@ -189,7 +210,7 @@
             self.c1[i].wait_recv()
             at = self.src((f + d) % 4, i)
             at[...] = (at[...].astype(jnp.float32) + got[...].astype(jnp.float32)).astype(jnp.bfloat16)
-            self.c2.append(self.net.copy(self.src((f + d) % 4), dst, self.dev((f + d) % 4, s)))
+            self.c2.append(self.net.copy(self.src((f + d) % 4), dst, self.dev((f + d) % 4, s), ss=self.out))
 
     def step3(self):
         f, s, w = self.f, self.s, self.wide
@@ -198,8 +219,8 @@
         total = self.src(f)[...].astype(jnp.float32) + self.rp[...].astype(jnp.float32)
         self.e[...] = (total + self.rm[...].astype(jnp.float32)).astype(self.kind)
         far = (s + 2) % 4
-        self.c3 = (self.net.copy(self.e.at[far, :, pl.ds(0, w)], self.ta, self.dev(f, (s + 1) % 4)),
-                   self.net.copy(self.e.at[far, :, pl.ds(w, w)], self.tb, self.dev(f, (s + 3) % 4)))
+        self.c3 = (self.net.copy(self.e.at[far, :, pl.ds(0, w)], self.ta, self.dev(f, (s + 1) % 4), ss=self.out),
+                   self.net.copy(self.e.at[far, :, pl.ds(w, w)], self.tb, self.dev(f, (s + 3) % 4), ss=self.out))
 
     def step4(self):
         f, s, w = self.f, self.s, self.wide
@@ -208,7 +229,7 @@
             self.c3[i].wait_recv()
             at = self.e.at[(s + d) % 4, :, pl.ds(i * w, w)]
             at[...] = (at[...].astype(jnp.float32) + got[...].astype(jnp.float32)).astype(self.kind)
-            self.c4.append(self.net.copy(self.e.at[(s + d) % 4], dst, self.dev(f, (s + d) % 4)))
+            self.c4.append(self.net.copy(self.e.at[(s + d) % 4], dst, self.dev(f, (s + d) % 4), ss=self.out))
 
     def step5(self):
         for x in self.c4:
@@ -227,7 +248,12 @@
 
 class Stream:
     def __init__(self, net, buf, slots):
-        self.routes = [Route(net, buf, 0, True, slots[:9]), Route(net, buf, 1, False, slots[9:])]
+        self.net, self.out = net, net.new_send()
+        self.blocks = 36 if slots[4].dtype == jnp.float32 else 30
+        self.routes = [Route(net, buf, 0, True, slots[:9], self.out), Route(net, buf, 1, False, slots[9:], self.out)]
+
+    def drain(self, flat):
+        self.net.wait_send(flat.at[pl.ds(0, self.blocks)], self.out)
 
     def run(self, name):
         return [getattr(r, name)() for r in self.routes]
@@ -268,10 +294,10 @@
             c.wait_recv()
 
 
-def whole_kernel(code_ref, lse_ref, pick_ref, q_hbm, k_hbm, v_hbm, o_hbm, do_hbm, x_hbm,
+def whole_kernel(chosen_ref, sums_ref, q_hbm, k_hbm, v_hbm, o_hbm, do_hbm, x_hbm,
                  dq_hbm, dk_hbm, dv_hbm, dw_ref, xall_hbm,
                  qb, kb, vb, ob, dob, dqt, dkb, dvb, dqb, delta_ref,
-                 need, rc, n1, ry, n2, rz, tab, pka, pva, pkb, pvb, gk, gv, part,
+                 need, names, lse_ref, pick_ref, square, codes, codes_s, tab, pka, pva, pkb, pvb, gk, gv, part,
                  info, spots, info_s, spots_s, to_s, rka, rva, rkb, rvb, ws, wr, wb, *rest):
     kas, vas, kbs, vbs, wslots = (rest[i * 18:i * 18 + 18] for i in range(5))
     send, recv, local = rest[90:]
@@ -281,12 +307,9 @@
     loads = [disk.copy(a, b) for a, b in
              ((k_hbm, kb), (v_hbm, vb), (q_hbm, qb), (do_hbm, dob), (o_hbm, ob))]
     partner = kv_of(z, y, 1 - c)
-    peers = [partner]
-    for d in range(1, 4):
-        peers += [kv_of(z, (y + d) % 4, c), kv_of((z + d) % 4, y, c)]
+    peers = [(me + d) % 32 for d in range(1, 32)]
     x = Ring(net, x_hbm, xall_hbm)
-    barrier_with(peers, x.t[1:3])
-
+    greet(peers, x.t[1:3])
     seqs, n, ch = qb.shape
     half = n // 2
 
@@ -298,25 +321,44 @@
     slots = 32 * CAP
     room = 18
 
+    for t in range(seqs):
+        v = chosen_ref[t]
+        there = v >> 3
+        codes[t, :, :12] = jnp.where((v >= 0) & (there != me), there * 128 + t * blocks + (v & 7), -1)
+    to_codes = disk.copy(codes, codes_s)
+    lse_ref[...] = sums_ref[...] * LOG2E
+    rep_rows = lax.broadcasted_iota(jnp.int32, (128, n), 0)
+    rep_cols = lax.broadcasted_iota(jnp.int32, (128, n), 1)
+    stretch = jnp.where(rep_rows == rep_cols // BLK, 1.0, 0.0).astype(jnp.bfloat16)
+    for t in range(seqs):
+        square[...] = jnp.full((128, 128), -1.0, jnp.float32)
+        square[:8, :12] = chosen_ref[t].astype(jnp.float32)
+        pick_ref[t] = mm(square[...].astype(jnp.bfloat16), stretch, TN)[:16]
     flat = (lax.broadcasted_iota(jnp.int32, (32, 128), 0) * 128 +
             lax.broadcasted_iota(jnp.int32, (32, 128), 1))
+    to_codes.wait()
 
     def mark(i, seen):
-        for j in range(8):
-            seen = jnp.where(flat == code_ref[i * 8 + j], 1, seen)
+        for j in range(12):
+            seen = jnp.where(flat == codes_s[i // 8, i % 8, j], 1, seen)
         return seen
 
-    seen = lax.fori_loop(0, code_ref.shape[0] // 8, mark, jnp.zeros((32, 128), jnp.int32))
+    seen = lax.fori_loop(0, 32, mark, jnp.zeros((32, 128), jnp.int32))
     for i in range(32):
-        need[i // 16, i // 4 % 4, i % 4] = jnp.broadcast_to(seen[i:i + 1], (8, 128))
-    first = net.copy(need.at[1 - c], rc, partner)
+        need[i] = seen[i:i + 1]
+    pl.semaphore_wait(pltpu.get_barrier_semaphore(), len(peers) + 2)
+    told, heard = net.new_send(), net.new_recv()
+    for d in range(1, 32):
+        to = (me + d) % 32
+        net.copy(need.at[to], names.at[me], to, ss=told, rs=heard)
+    names[me] = jnp.zeros((1, 128), jnp.int32)
     x.start()
     for l in loads:
         l.wait()
 
     def bias_row(lse, s, block):
-        hit = jnp.max(jnp.where(pick_ref[s] == block, 1, 0), axis=0, keepdims=True)
-        return jnp.where(hit > 0, lse, BIG)
+        hit = jnp.max(jnp.where(pick_ref[s] == jnp.asarray(block, jnp.float32), 1.0, 0.0), axis=0, keepdims=True)
+        return jnp.where(hit > 0.5, lse, BIG)
 
     def unit(u, _):
         s = u // 2
@@ -358,18 +400,8 @@
         lax.fori_loop(a, b, unit, 0)
 
     units(0, 1)
-    first.wait_recv()
-    n1[...] = jnp.maximum(need[c], rc[...])
-    ys = [net.copy(n1.at[(y + d) % 4], ry.at[d - 1], kv_of(z, (y + d) % 4, c)) for d in range(1, 4)]
-    units(1, 2)
-    for a in ys:
-        a.wait_recv()
-    n2[...] = jnp.maximum(jnp.maximum(n1[y], ry[0]), jnp.maximum(ry[1], ry[2]))
-    zs = [net.copy(n2.at[(z + d) % 4], rz.at[d - 1], kv_of((z + d) % 4, y, c)) for d in range(1, 4)]
-    units(2, 3)
-    for a in zs:
-        a.wait_recv()
-    need1 = jnp.maximum(jnp.maximum(n2[z], rz[0]), jnp.maximum(rz[1], rz[2]))
+    net.wait_recv(names.at[pl.ds(0, 31)], heard)
+    need1 = jnp.broadcast_to(jnp.max(names[...], axis=0), (8, 128))
     info[...] = need1
     disk.copy(info, info_s).wait()
 
@@ -409,18 +441,18 @@
             getattr(g, name)(*j)
 
     each(ga, "phase0")
-    units(3, 5)
+    units(1, 3)
     for a in tys:
         a.wait_recv()
     tzs = [net.copy(tab.at[c, z], tab.at[c, z], kv_of((z + d) % 4, y, c)) for d in range(1, 4)]
     each(ga, "phase1")
-    units(5, 6)
+    units(3, 5)
     each(ga, "phase2")
     each(gb, "phase0")
     for a in tzs:
         a.wait_recv()
     tside = net.copy(tab.at[c], tab.at[c], partner)
-    units(6, 7)
+    units(5, 7)
     each(ga, "phase3", 0)
     each(ga, "phase3", 1)
     each(gb, "phase1")
@@ -566,7 +598,8 @@
     x.pass_on(0)
     first_half(9, room)
     each(gb, "phase5")
-    each(ga, "drain")
+    ga[0].drain(pka)
+    ga[1].drain(pva)
     settle(0)
     side_va = side(pva, rva)
     side_ka = side(pka, rka)
@@ -587,7 +620,8 @@
     second_half(10, 14)
     va.run("step3")
     second_half(14, room)
-    each(gb, "drain")
+    gb[0].drain(pkb)
+    gb[1].drain(pvb)
     settle(1)
     side_vb = side(pvb, rvb)
     side_kb = side(pkb, rkb)
@@ -599,9 +633,8 @@
     ksb = Stream(net, six(pkb).at[c], kbs)
     fold(pvb, rvb, side_vb)
     vsb.run("step1")
+    ka.run("step4")
     fold(pkb, rkb, side_kb)
-    ksb.run("step1")
-    ka.run("step4")
 
     x.near()
     load_x = [own_x, disk.copy(xall_hbm.at[x.t[1]], vb), disk.copy(xall_hbm.at[x.t[2]], ob)]
@@ -624,13 +657,14 @@
 
     product(0)
     vsb.run("step2")
+    ksb.run("step1")
     fva = va.run("step5")
     product(1)
-    ksb.run("step2")
     fka = ka.run("step5")
     vsb.run("step3")
     product(2)
     vsb.run("step4")
+    ksb.run("step2")
     x.far()
     dq_out.wait()
     load_x.append(disk.copy(xall_hbm.at[x.t[3]], dqb))
@@ -681,14 +715,16 @@
     top, low = w.run("step5")
     dw_ref[:BLK // 2] = top
     dw_ref[BLK // 2:] = low
-    done = set(id(a) for g in ga + gb for a in g.sent)
-    for a in net.all:
-        if id(a) not in done:
-            a.wait_send()
+    for st, ref in ((va, pva), (ka, pva), (vsb, pva), (ksb, pva), (w, pva)):
+        st.drain(ref)
+    net.wait_send(names.at[pl.ds(0, 31)], told)
+    net.finish()
     disk.finish()
-
-
-def fused(code, lse, pick, q, k, v, o, do, x):
+    assert net.n <= RECVS and net.ns <= SENDS, (net.n, net.ns)
+    assert disk.n <= 16, disk.n
+
+
+def fused(chosen, sums, q, k, v, o, do, x):
     seqs, n, ch = q.shape
     blk = k.shape
     heads = ch // DH
@@ -699,7 +735,7 @@
     V = pltpu.VMEM
     return pl.pallas_call(
         whole_kernel,
-        in_specs=[pl.BlockSpec(memory_space=pltpu.SMEM)] + [whole] * 2 + [hbm] * 6,
+        in_specs=[whole] * 2 + [hbm] * 6,
         out_specs=[hbm] * 3 + [whole, hbm],
         out_shape=[
             jax.ShapeDtypeStruct(blk, bf),
@@ -710,8 +746,8 @@
         ],
         scratch_shapes=[V(q.shape, bf)] + [V(blk, bf)] * 3 + [V(q.shape, bf), V((seqs, ch, n), f32)] + [V(blk, bf)] * 3 + [
             V((seqs, heads, n), f32),
-            V((2, 4, 4, 8, 128), i32), V((4, 4, 8, 128), i32), V((4, 4, 8, 128), i32),
-            V((3, 4, 8, 128), i32), V((4, 8, 128), i32), V((3, 8, 128), i32), V((2, 4, 4, 8, 128), i32),
+            V((32, 1, 128), i32), V((32, 1, 128), i32), V((seqs, heads, n), f32), V((seqs, 16, n), f32),
+            V((128, 128), f32), V((4, 8, 128), i32), pltpu.SMEM((4, 8, 128), i32), V((2, 4, 4, 8, 128), i32),
             V((64, BLK, wide), bf), V((64, BLK, wide), bf), V((64, BLK, wide), bf), V((64, BLK, wide), bf),
             V((73, BLK, wide), bf), V((73, BLK, wide), bf), V((36, DH, n), f32),
             V((8, 128), i32), V((32, 128), i32),
@@ -720,33 +756,26 @@
             V((16, BLK, ch), bf), V((16, BLK, ch), bf), V((4, 4, 2, BLK // 2, ch), bf),
         ] + (route_scratch(BLK, wide, bf) * 2 + route_scratch(BLK, wide, f32) * 2) * 2
         + route_scratch(BLK // 2, ch, f32) * 2 + [
-            pltpu.SemaphoreType.DMA((256,)), pltpu.SemaphoreType.DMA((256,)), pltpu.SemaphoreType.DMA((20,)),
+            pltpu.SemaphoreType.DMA((SENDS,)), pltpu.SemaphoreType.DMA((RECVS,)), pltpu.SemaphoreType.DMA((16,)),
         ],
         compiler_params=pltpu.CompilerParams(
             vmem_limit_bytes=67043328, collective_id=0, has_side_effects=True),
         cost_estimate=pl.CostEstimate(flops=20_000_000_000, bytes_accessed=30 << 20, transcendentals=1 << 22),
         name="fused_backward",
-    )(code, lse, pick, q, k, v, o, do, x)
+    )(chosen, sums, q, k, v, o, do, x)
 
 
 def body(layer_input, queries, keys, values, outputs, d_out, log_sums, chosen):
     seqs, n, ch = queries.shape
     blocks = n // BLK
     me = lax.axis_index("kv")
-    lse = jnp.swapaxes(log_sums, 1, 2) * LOG2E
-    owner = chosen // blocks
-    row = (owner % 2) * 16 + (owner // 2 % 4) * 4 + owner // 8
-    lane = jnp.arange(seqs, dtype=jnp.int32)[:, None, None] * blocks + chosen % blocks
-    code = jnp.where((chosen >= 0) & (owner != me), row * 128 + lane, -1).reshape(-1)
-    pick = jnp.swapaxes(chosen, 1, 2)
-    pick = jnp.pad(pick, ((0, 0), (0, 16 - pick.shape[1]), (0, 0)), constant_values=-1)
-    pick = jnp.repeat(pick, BLK, axis=2)
-
     def cut(a):
         return a.reshape(seqs, blocks, BLK, ch)
 
-    dq, dk, dv, dw, _ = fused(code, lse, pick, queries, cut(keys), cut(values), cut(outputs), d_out, cut(layer_input))
-    return dq.reshape(queries.shape), dk.reshape(queries.shape), dv.reshape(queries.shape), dw
+    dq, dk, dv, dw, _ = fused(chosen, jnp.swapaxes(log_sums, 1, 2), queries, cut(keys), cut(values),
+                              cut(outputs), d_out, cut(layer_input))
+    return tuple(jnp.where(me >= 0, a, jnp.zeros_like(a)).reshape(shape) for a, shape in
+                 ((dq, queries.shape), (dk, queries.shape), (dv, queries.shape), (dw, dw.shape)))
 
 
 def solution(mesh):

time: 141 us -> 127 us (0.901)
  local copies, waits for them, and re-layouts: 9.93 us -> 0.01 us
  Pallas kernels: 128 us -> 119 us
  other arithmetic: 2.18 us -> 6.78 us
    pallas_call x1, Pallas kernels: 128 us -> 119 us  [fused(): pl.pallas_call(whole_kernel, in_specs=[whole] * 2 + [hbm] * 6, out_specs=...]
    unnamed x11 -> x4, local copies, waits for them, and re-layouts: 8.34 us -> 0.01 us
    select_n x1 -> x3, other arithmetic: 0.8 us -> 6.78 us  [body(): jnp.where(me >= 0, a, jnp.zeros_like(a)).reshape(shape)]
    reshape x2 -> x0, local copies, waits for them, and re-layouts: 1.46 us -> none  [the longest x1 0.77 us: body(): pick = jnp.repeat(pick, BLK, axis=2)]
where the time goes in v4:
time: 127 us; the launch traced here: 126 us
  Pallas kernels  119 us (94%)
  other arithmetic  6.78 us (5%)
    pallas_call x1, Pallas kernels, fused(): pl.pallas_call(whole_kernel, in_specs=[whole] * 2 + [hbm] * 6, out_specs=...  119 us
    select_n x3, other arithmetic, body(): jnp.where(me >= 0, a, jnp.zeros_like(a)).reshape(shape)  6.78 us

profile of v4, /device:TPU:0, one launch (start us, length us, event | category | flops | bytes accessed | tf_op | source)
XLA Modules:
  0.0 126.5 jit_solution(14208511906076431555)
XLA Ops:
  0.6 119.0 %fused_backward.1 = (bf16[4,8,64,512]{3,2,1,0:T(8,128)(2,1)}, bf16[4,8,64,512]{3,2,1,0:T(8,128)(2,1)}, bf16[4,8,64,512]{3,2,1,0:T(8,128)(2,1)}, f32[64,512]{1,0:T(8,128)}, bf16[4,4,8,64,512]{4,3,2,1,0:T(8,128)(2,1)}) custom-call(s32[4,8,12]{2,1,0:T(8,128)} %chosen_ref.1, f32[4,4,512]{2,1,0:T(4,128)} %bitcast.15, bf16[4,512,512]{2,1,0:T(8,128)(2,1)} %q_hbm.1, ...), custom_call_target="tpu_custom_call" | custom-call | flops 20000000000 | bytes 31457280 | tf_op jit(solution)/shard_map/fused_backward/pallas_call | solution.py:736
  119.7 0.0 copy-start
  119.7 4.7 %broadcast_select_fusion = (bf16[4,8,64,512]{3,2,1,0:T(8,128)(2,1)}, bf16[4,8,64,512]{3,2,1,0:T(8,128)(2,1)}) fusion(bf16[4,8,64,512]{3,2,1,0:T(8,128)(2,1)} %get-tuple-element.10, pred[]{:T(512)S(6)} %ge.2, bf16[4,8,64,512]{3,2,1,0:T(8,128)(2,1)} %get-tuple-element.9), kind=kLoop, calls=%fused_computation | loop fusion | flops 2097152 | bytes 8388609 | tf_op jit(solution)/shard_map/jit(_where)/select_n | solution.py:777
  124.3 0.0 copy-done
  124.3 0.0 copy-start.1
  124.3 1.5 %broadcast_select_fusion.2 = bf16[4,8,64,512]{3,2,1,0:T(8,128)(2,1)} fusion(bf16[4,8,64,512]{3,2,1,0:T(8,128)(2,1)S(1)} %copy-done, pred[]{:T(512)S(6)} %ge.2), kind=kLoop, calls=%fused_computation.2 | loop fusion | flops 1048576 | bytes 4194305 | tf_op jit(solution)/shard_map/jit(_where)/select_n | solution.py:777
  125.8 0.0 copy-done.1
  125.8 0.7 broadcast_select_fusion.3
Async XLA Ops:
  119.7 4.7 %copy-start = (bf16[4,8,64,512]{3,2,1,0:T(8,128)(2,1)S(1)}, bf16[4,8,64,512]{3,2,1,0:T(8,128)(2,1)}, u32[]{:S(2)}) copy-start(bf16[4,8,64,512]{3,2,1,0:T(8,128)(2,1)} %get-tuple-element.8) | copy-start | bytes 6291460
  124.3 1.5 %copy-start.1 = (f32[64,512]{1,0:T(8,128)S(1)}, f32[64,512]{1,0:T(8,128)}, u32[]{:S(2)}) copy-start(f32[64,512]{1,0:T(8,128)} %get-tuple-element.11) | copy-start | bytes 393220

commit v5 on v4

--- a/solution.py
+++ b/solution.py
@@ -356,12 +356,12 @@
     for l in loads:
         l.wait()
 
-    def bias_row(lse, s, block):
-        hit = jnp.max(jnp.where(pick_ref[s] == jnp.asarray(block, jnp.float32), 1.0, 0.0), axis=0, keepdims=True)
-        return jnp.where(hit > 0.5, lse, BIG)
+    def hit_row(s, block):
+        return jnp.max(jnp.where(pick_ref[s] == jnp.asarray(block, jnp.float32), 1.0, 0.0), axis=0, keepdims=True)
 
     def unit(u, _):
         s = u // 2
+        hits = [hit_row(s, me * blocks + j) for j in range(blocks)]
         for g in range(2):
             h = (u % 2) * 2 + g
             hs = pl.ds(pl.multiple_of(h * DH, DH), DH)
@@ -384,7 +384,7 @@
                 row = lax.broadcasted_iota(jnp.int32, (half, w), 0)
                 col = lax.broadcasted_iota(jnp.int32, (half, w), 1)
                 bias = jnp.concatenate(
-                    [jnp.broadcast_to(bias_row(lse, s, me * blocks + j)[:, lo:], (BLK, w))
+                    [jnp.broadcast_to(jnp.where(hits[j] > 0.5, lse, BIG)[:, lo:], (BLK, w))
                      for j in range(lo // BLK, (lo + half) // BLK)], axis=0)
                 p = jnp.exp2(jnp.where(row <= col, sc * (ROOT * LOG2E) - bias, -BIG))
                 dp = mm(v, doc, NT)
@@ -524,6 +524,7 @@
             keep = jnp.where((s == seq_of(i - 1)) & (i > 0), 1, 0)
             keep = jnp.broadcast_to(keep, (1, n)) == 1
             who = [(jnp.clip(info_s[0, 4 * i + e], 0, slots - 1), info_s[1, 4 * i + e]) for e in range(4)]
+            hits = [hit_row(s, b) for _, b in who]
             for g in range(2):
                 h = 2 * second + g
                 gs = slice(g * DH, (g + 1) * DH)
@@ -535,7 +536,7 @@
                 lse = lse_ref[s, h:h + 1, :]
                 st = mm(k, q, NT)
                 bias = jnp.concatenate(
-                    [jnp.broadcast_to(bias_row(lse, s, b), (BLK, n)) for _, b in who], axis=0)
+                    [jnp.broadcast_to(jnp.where(b > 0.5, lse, BIG), (BLK, n)) for b in hits], axis=0)
                 p = jnp.exp2(st * (ROOT * LOG2E) - bias)
                 dp = mm(v, do, NT)
                 ds = (p * (dp - delta_ref[s, h:h + 1, :])).astype(jnp.bfloat16)
@@ -586,17 +587,21 @@
         lax.fori_loop(0, 32, add, 0)
 
     first_half = attend(0)
-    first_half(0, 3)
     each(gb, "phase3", 0)
+    first_half(0, 2)
     each(gb, "phase3", 1)
-    first_half(3, 6)
+    first_half(2, 4)
     each(gb, "phase3", 2)
+    first_half(4, 6)
     each(gb, "phase3", 3)
     first_half(6, 9)
-    for j in range(4):
+    for j in range(2):
+        each(gb, "phase4", j)
+    first_half(9, 12)
+    for j in range(2, 4):
         each(gb, "phase4", j)
     x.pass_on(0)
-    first_half(9, room)
+    first_half(12, room)
     each(gb, "phase5")
     ga[0].drain(pka)
     ga[1].drain(pva)
@@ -765,6 +770,40 @@
     )(chosen, sums, q, k, v, o, do, x)
 
 
+def hand_kernel(*refs):
+    n = 4
+    src, dst, buf, sems_in, sems_out = refs[:n], refs[n:2 * n], refs[2 * n:3 * n], refs[3 * n], refs[3 * n + 1]
+    parts = [(a, p) for p in range(4) for a in range(n) if a < 3 or p == 0]
+
+    def at(ref, a, p):
+        return ref.at[p] if a < 3 else ref
+
+    loads, stores = [], []
+    for i, (a, p) in enumerate(parts):
+        loads.append(pltpu.make_async_copy(at(src[a], a, p), at(buf[a], a, p), sems_in.at[i]))
+        loads[-1].start()
+    for i, (a, p) in enumerate(parts):
+        loads[i].wait()
+        stores.append(pltpu.make_async_copy(at(buf[a], a, p), at(dst[a], a, p), sems_out.at[i]))
+        stores[-1].start()
+    for c in stores:
+        c.wait()
+
+
+def hand_over(*arrays):
+    hbm = pl.BlockSpec(memory_space=pl.ANY)
+    return pl.pallas_call(
+        hand_kernel,
+        in_specs=[hbm] * 4,
+        out_specs=[hbm] * 4,
+        out_shape=[jax.ShapeDtypeStruct(a.shape, a.dtype) for a in arrays],
+        scratch_shapes=[pltpu.VMEM(a.shape, a.dtype) for a in arrays] + [
+            pltpu.SemaphoreType.DMA((13,)), pltpu.SemaphoreType.DMA((13,))],
+        compiler_params=pltpu.CompilerParams(vmem_limit_bytes=60 * 1024 * 1024),
+        name="hand_over",
+    )(*arrays)
+
+
 def body(layer_input, queries, keys, values, outputs, d_out, log_sums, chosen):
     seqs, n, ch = queries.shape
     blocks = n // BLK
@@ -774,8 +813,8 @@
 
     dq, dk, dv, dw, _ = fused(chosen, jnp.swapaxes(log_sums, 1, 2), queries, cut(keys), cut(values),
                               cut(outputs), d_out, cut(layer_input))
-    return tuple(jnp.where(me >= 0, a, jnp.zeros_like(a)).reshape(shape) for a, shape in
-                 ((dq, queries.shape), (dk, queries.shape), (dv, queries.shape), (dw, dw.shape)))
+    dq, dk, dv, dw = hand_over(dq, dk, dv, dw)
+    return dq.reshape(queries.shape), dk.reshape(queries.shape), dv.reshape(queries.shape), dw
 
 
 def solution(mesh):

time: 127 us -> 124 us (0.976)
  other arithmetic: 6.78 us -> 0 us
  Pallas kernels: 119 us -> 122 us
    select_n x3 -> x0, other arithmetic: 6.78 us -> none  [body(): jnp.where(me >= 0, a, jnp.zeros_like(a)).reshape(shape)]
    pallas_call x0 -> x1, Pallas kernels: none -> 5.57 us  [hand_over(): pl.pallas_call(hand_kernel, in_specs=[hbm] * 4, out_specs=[hbm] * 4, out_...]
    pallas_call x1, Pallas kernels: 119 us -> 117 us  [fused(): pl.pallas_call(whole_kernel, in_specs=[whole] * 2 + [hbm] * 6, out_specs=...]
where the time goes in v5:
time: 124 us; the launch traced here: 123 us
  Pallas kernels  122 us (98%)
    pallas_call x1, Pallas kernels, fused(): pl.pallas_call(whole_kernel, in_specs=[whole] * 2 + [hbm] * 6, out_specs=...  117 us
    pallas_call x1, Pallas kernels, hand_over(): pl.pallas_call(hand_kernel, in_specs=[hbm] * 4, out_specs=[hbm] * 4, out_...  5.57 us

profile of v5, /device:TPU:0, one launch (start us, length us, event | category | flops | bytes accessed | tf_op | source)
XLA Modules:
  0.0 123.3 jit_solution(4452867456642417188)
XLA Ops:
  0.6 116.9 %fused_backward.1 = (bf16[4,8,64,512]{3,2,1,0:T(8,128)(2,1)}, bf16[4,8,64,512]{3,2,1,0:T(8,128)(2,1)}, bf16[4,8,64,512]{3,2,1,0:T(8,128)(2,1)}, f32[64,512]{1,0:T(8,128)}, bf16[4,4,8,64,512]{4,3,2,1,0:T(8,128)(2,1)}) custom-call(s32[4,8,12]{2,1,0:T(8,128)} %chosen_ref.1, f32[4,4,512]{2,1,0:T(4,128)} %bitcast.15, bf16[4,512,512]{2,1,0:T(8,128)(2,1)} %q_hbm.1, ...), custom_call_target="tpu_custom_call" | custom-call | flops 20000000000 | bytes 31457280 | tf_op jit(solution)/shard_map/fused_backward/pallas_call | solution.py:741
  117.6 5.6 %hand_over.1 = (bf16[4,8,64,512]{3,2,1,0:T(8,128)(2,1)}, bf16[4,8,64,512]{3,2,1,0:T(8,128)(2,1)}, bf16[4,8,64,512]{3,2,1,0:T(8,128)(2,1)}, f32[64,512]{1,0:T(8,128)}) custom-call(bf16[4,8,64,512]{3,2,1,0:T(8,128)(2,1)} %get-tuple-element.12.refs_0_, bf16[4,8,64,512]{3,2,1,0:T(8,128)(2,1)} %get-tuple-element.13.refs_1_, ...), custom_call_target="tpu_custom_call" | custom-call | tf_op jit(solution)/shard_map/hand_over/pallas_call | solution.py:795
